TPU v7x, 32 devices: a whole 2x2x4 slice. The times are simulated.
32 devices in a mesh: sp: 16 (over z, y, core), tp: 2 (over x).
Axes of the slice: x: 2, y: 2, z: 4, core: 2. Of those that a mesh axis runs over, the one named last changes fastest.
Arguments:
- tokens: bfloat16 [16384, 2048], P('sp'), may hold values from -6 to 6
- norm_gain: float32 [2048], replicated, may hold values from 0.1 to 1.9
- w_query: bfloat16 [2048, 512], P(None, 'tp'), may hold values from -0.79549513 to 0.79549513
- w_key: bfloat16 [2048, 128], P('sp'), may hold values from -0.79549513 to 0.79549513
- w_value: bfloat16 [2048, 128], P('sp'), may hold values from -0.125 to 0.125
- w_pool_in: bfloat16 [2048, 512], P(None, 'tp'), may hold values from -0.125 to 0.125
- sink_logit: float32 [8], P('tp'), may hold values from 3 to 7
- pool_scale: float32 [512], P('tp'), may hold values from 0.05 to 0.5
- w_out: bfloat16 [1024, 2048], P('tp', 'sp'), may hold values from -0.75 to 0.75
Outputs:
- mixed_out: bfloat16 [16384, 2048], P(('sp', 'tp'))
All inputs are finite; a program needn't handle non-finite values.
Results may differ from a plain program's by a relative error of at most 0.03.
The roundings to bfloat16 on the way count: a program that leaves them out, or rounds other values in their place, can miss the bound.
Values may be sent and summed in bfloat16 or wider, within the bound.
A program may use at most 64 MiB of HBM per device.

v0:
```python
import functools

import jax
import jax.numpy as jnp
from jax import lax
from jax.experimental import pallas as pl
from jax.experimental.pallas import tpu as pltpu
from jax.sharding import PartitionSpec as P

HEAD = 64
QH = 8
KVH = 2
POOL_CH = 128
WINDOW = 128
QB = 128


NEG_BIG = -1e30
POOL_SPANS = (2, 4, 8, 16)


def extended(block, sides, width):
    for axis, dim in sides:
        count = lax.axis_size(axis)
        forward = [(i, i + 1) for i in range(count - 1)]
        backward = [(target, source) for source, target in forward]
        low = lax.ppermute(
            lax.slice_in_dim(block, block.shape[dim] - width, None, axis=dim), axis, forward
        )
        high = lax.ppermute(lax.slice_in_dim(block, 0, width, axis=dim), axis, backward)
        block = jnp.concatenate([low, block, high], axis=dim)
    return block


def layer_normed(tokens, norm_gain):
    values = tokens.astype(jnp.float32)
    center = jnp.mean(values, axis=-1, keepdims=True)
    spread = jnp.mean(jnp.square(values - center), axis=-1, keepdims=True)
    return ((values - center) * lax.rsqrt(spread + 1e-06) * norm_gain).astype(jnp.bfloat16)


def rotate(values, positions):
    half = HEAD // 2
    inverse = 10000.0 ** (-jnp.arange(half, dtype=jnp.float32) / half)
    angles = positions[:, None] * inverse[None, :]
    cosine = jnp.cos(angles)[:, None, :]
    sine = jnp.sin(angles)[:, None, :]
    first = values[..., :half]
    second = values[..., half:]
    return jnp.concatenate(
        [first * cosine - second * sine, first * sine + second * cosine], axis=-1
    )


def plain_body(tokens, norm_gain, w_query, w_key, w_value, w_pool_in, sink_logit, pool_scale, w_out):
    local_rows = tokens.shape[0]
    seq_total = local_rows * lax.axis_size("sp")
    offset = lax.axis_index("sp") * local_rows
    tp_place = lax.axis_index("tp")
    local_heads = w_query.shape[1] // HEAD
    local_pool = w_pool_in.shape[1]
    reach = POOL_SPANS[-1] // 2
    normed = layer_normed(tokens, norm_gain)
    positions = (offset + jnp.arange(local_rows)).astype(jnp.float32)
    query = rotate(
        jnp.dot(normed, w_query, preferred_element_type=jnp.float32).reshape(
            local_rows, local_heads, HEAD
        ),
        positions,
    ).astype(jnp.bfloat16)
    key_head = tp_place * local_heads // (QH // KVH)
    key_cols = lax.dynamic_slice_in_dim(w_key, key_head * HEAD, HEAD, 1)
    value_cols = lax.dynamic_slice_in_dim(w_value, key_head * HEAD, HEAD, 1)
    key_sum = jnp.dot(
        normed,
        lax.all_gather(key_cols, "sp", axis=0, tiled=True),
        preferred_element_type=jnp.float32,
    )
    value_sum = jnp.dot(
        normed,
        lax.all_gather(value_cols, "sp", axis=0, tiled=True),
        preferred_element_type=jnp.float32,
    )
    key = rotate(key_sum[:, None, :], positions)[:, 0, :].astype(jnp.bfloat16)
    value = value_sum.astype(jnp.bfloat16)
    key_value = jnp.concatenate([key, value], axis=1)
    pool_in = jnp.dot(normed, w_pool_in, preferred_element_type=jnp.float32).astype(jnp.bfloat16)
    widened = extended(jnp.concatenate([key_value, pool_in], axis=1), (("sp", 0),), WINDOW)
    kv_wide = widened[:, : 2 * HEAD]
    pool_wide = widened[WINDOW - reach : WINDOW + local_rows + reach, 2 * HEAD :]
    span = QB + 2 * WINDOW
    sink_here = sink_logit[:, None, None]
    results = []
    for block in range(local_rows // QB):
        queries = query[block * QB : (block + 1) * QB]
        keys = kv_wide[block * QB : block * QB + span, :HEAD]
        values = kv_wide[block * QB : block * QB + span, HEAD:]
        scores = jnp.einsum(
            "ihd,jd->hij", queries, keys, preferred_element_type=jnp.float32
        ) * HEAD ** (-0.5)
        query_pos = offset + block * QB + jnp.arange(QB)
        key_pos = offset + block * QB - WINDOW + jnp.arange(span)
        valid = (
            (jnp.abs(query_pos[:, None] - key_pos[None, :]) <= WINDOW)
            & (key_pos[None, :] >= 0)
            & (key_pos[None, :] < seq_total)
        )
        scores = jnp.where(valid, scores, NEG_BIG)
        highest = jnp.maximum(jnp.max(scores, axis=-1, keepdims=True), sink_here)
        expo = jnp.where(valid, jnp.exp(scores - highest), 0.0)
        total = jnp.sum(expo, axis=-1, keepdims=True) + jnp.exp(sink_here - highest)
        weights = (expo / total).astype(jnp.bfloat16)
        result = jnp.einsum("hij,jd->ihd", weights, values, preferred_element_type=jnp.float32)
        results.append(result.reshape(QB, local_heads * HEAD).astype(jnp.bfloat16))
    attended = jnp.concatenate(results, axis=0)
    pool_vals = pool_wide.astype(jnp.float32)
    window_sum = pool_vals
    global_pos = offset + jnp.arange(local_rows)
    channel = tp_place * local_pool + jnp.arange(local_pool)
    window_group = channel // POOL_CH
    measured = jnp.zeros((local_rows, local_pool), jnp.float32)
    stride = 1
    for index, width in enumerate(POOL_SPANS):
        window_sum = window_sum[:-stride] + window_sum[stride:]
        stride = width
        sums = window_sum[reach - width // 2 : reach - width // 2 + local_rows]
        counted = (
            jnp.minimum(global_pos + width // 2, seq_total)
            - jnp.maximum(global_pos - width // 2, 0)
        ).astype(jnp.float32)
        measured = measured + jnp.where(
            window_group[None, :] == index, sums / counted[:, None], 0.0
        )
    pooled = ((measured - pool_vals[reach : reach + local_rows]) * pool_scale).astype(jnp.bfloat16)
    attended_rows, pooled_rows = (
        lax.all_to_all(attended, "tp", split_axis=0, concat_axis=1, tiled=True),
        lax.all_to_all(pooled, "tp", split_axis=0, concat_axis=1, tiled=True),
    )
    joined = jnp.concatenate([attended_rows, pooled_rows], axis=1)
    out_rows_all = lax.all_gather(w_out, "tp", axis=0, tiled=True)
    projected = jnp.dot(
        joined,
        lax.all_gather(out_rows_all, "sp", axis=1, tiled=True),
        preferred_element_type=jnp.float32,
    )
    return projected.astype(jnp.bfloat16)


LANES = 128
CHUNK = 256
MESH = pl.DeviceIdType.MESH


def rope_tables(offset, rows):
    half = HEAD // 2
    inverse = 10000.0 ** (-jnp.arange(half, dtype=jnp.float32) / half)
    inverse = jnp.tile(inverse, LANES // half)[None, :]
    sign = jnp.where(jnp.arange(LANES) % HEAD < half, -1.0, 1.0)[None, :]
    inner = jnp.arange(QB, dtype=jnp.float32)[:, None] * inverse
    starts = (offset + QB * jnp.arange(rows // QB)).astype(jnp.float32)[:, None] * inverse
    return jnp.cos(inner), jnp.sin(inner) * sign, jnp.cos(starts), jnp.sin(starts) * sign


def mixer_kernel(
    places, tokens, gain, w_query, kv_block, w_pool, sink, scale, w_out, cos_in, sin_in, cos_at, sin_at,
    out,
    tok, normed, wq, wp, kvw, wfull, qs, kv, pool, pool_send, att_send, joined, out_v,
    tok_sem, own_sem, out_sem, kv_send, kv_recv, kvf_send, wx_send, wx_recv, wo_send, wo_recv,
    wf_send, wp_send, halo_send, halo_recv, ex_send, ex_recv,
):
    S, T = places
    Z = S // 4
    s = lax.axis_index("sp")
    t = lax.axis_index("tp")
    rows = tokens.shape[0]
    width = tokens.shape[1]
    blocks = rows // QB
    hb = blocks // 2
    chunks = rows // CHUNK
    local_heads = w_query.shape[1] // HEAD
    groups = w_query.shape[1] // LANES
    pgroups = w_pool.shape[1] // LANES
    reach = POOL_SPANS[-1] // 2
    offset = s * rows
    total_rows = S * rows
    c = s % 2
    y = (s // 2) % 2
    z = s // 4
    quad = s % 4
    partner = s + 1 - 2 * c
    yflip = s + 2 - 4 * y
    after = (s + 1) % S
    before = (s + S - 1) % S
    cross = 1 - t
    hops = sorted(range(1, Z), key=lambda d: (min(d, Z - d), d))

    def zmate(d, base):
        return ((z + d) % Z) * 4 + base % 4

    def remote(a, b, send, recv, to_s, to_t):
        return pltpu.make_async_remote_copy(
            src_ref=a, dst_ref=b, send_sem=send, recv_sem=recv,
            device_id={"sp": to_s, "tp": to_t}, device_id_type=MESH,
        )

    same_core = [zmate(d, s) for d in hops] + [zmate(d, yflip) for d in range(Z)]

    tok_copies = [
        pltpu.make_async_copy(
            tokens.at[pl.ds(i * CHUNK, CHUNK)], tok.at[pl.ds(i * CHUNK, CHUNK)], tok_sem.at[i]
        )
        for i in range(chunks)
    ]
    tok_copies[0].start()
    own_copies = [
        pltpu.make_async_copy(w_query, wq, own_sem.at[0]),
        pltpu.make_async_copy(w_pool, wp, own_sem.at[1]),
        pltpu.make_async_copy(kv_block, kvw.at[s], own_sem.at[2]),
        pltpu.make_async_copy(w_out, wfull.at[s, t], own_sem.at[3]),
    ]
    for copy in own_copies:
        copy.start()
    for copy in tok_copies[1:]:
        copy.start()

    barrier = pltpu.get_barrier_semaphore()
    greet = [(b, t) for b in same_core + [after, before]] + [(s, cross)]
    for to_s, to_t in greet:
        pl.semaphore_signal(barrier, inc=1, device_id={"sp": to_s, "tp": to_t}, device_id_type=MESH)
    pl.semaphore_wait(barrier, len(greet))

    kv_copies = [
        remote(kv_block, kvw.at[s], kv_send.at[i], kv_recv.at[s], b, t)
        for i, b in enumerate(same_core)
    ]
    for copy in kv_copies:
        copy.start()
    x_copy = remote(w_out, wfull.at[s, t], wx_send, wx_recv, s, cross)
    x_copy.start()
    x_in = remote(w_out, wfull.at[s, cross], wx_send, wx_recv, s, cross)

    kv_forward = [
        remote(kvw.at[b], kvw.at[b], kvf_send.at[i], kv_recv.at[b], partner, t)
        for i, b in enumerate([s] + same_core)
    ]
    wo_to = [zmate(d, s) for d in hops] + [yflip, partner]
    wo_own = [
        remote(w_out, wfull.at[s, t], wo_send.at[0, i], wo_recv.at[s, t], b, t)
        for i, b in enumerate(wo_to)
    ]
    wo_crossed = [
        remote(wfull.at[s, cross], wfull.at[s, cross], wo_send.at[1, i], wo_recv.at[s, cross], b, t)
        for i, b in enumerate(wo_to)
    ]
    for copy in wo_own:
        copy.start()

    def z_copies(i, k):
        b = zmate(hops[i], s)
        half = cross if k else t
        piece = wfull.at[b, half]
        return [
            remote(piece, piece, wf_send.at[k, 2 * i + j], wo_recv.at[b, half], to, t)
            for j, to in enumerate([yflip, partner])
        ]

    def y_copy(d, k):
        b = zmate(d, yflip)
        half = cross if k else t
        piece = wfull.at[b, half]
        return remote(piece, piece, wp_send.at[k, d], wo_recv.at[b, half], partner, t)

    def forward_z(i, k):
        copies = z_copies(i, k)
        copies[0].wait_recv()
        for copy in copies:
            copy.start()

    def forward_y(d, k):
        copy = y_copy(d, k)
        copy.wait_recv()
        copy.start()

    lane = lax.broadcasted_iota(jnp.int32, (QB, LANES), 1)
    low_half = lane < HEAD
    first_half = lane % HEAD < HEAD // 2

    def rotated(values, b):
        ca = cos_at[pl.ds(b, 1), :]
        sa = sin_at[pl.ds(b, 1), :]
        ci = cos_in[...]
        si = sin_in[...]
        cosine = ca * ci - sa * si
        sine = sa * ci + ca * si
        swapped = jnp.where(
            first_half,
            pltpu.roll(values, LANES - HEAD // 2, 1),
            pltpu.roll(values, HEAD // 2, 1),
        )
        return values * cosine + swapped * sine

    own_copies[0].wait()
    own_copies[1].wait()
    LN = 32

    def project(i, carry):
        base = pl.multiple_of(i * CHUNK, CHUNK)
        pltpu.make_async_copy(
            tokens.at[pl.ds(base, CHUNK)], tok.at[pl.ds(base, CHUNK)], tok_sem.at[i]
        ).wait()

        def norm(r, carry):
            at = pl.multiple_of(base + r * LN, LN)
            values = tok[pl.ds(at, LN), :].astype(jnp.float32)
            center = jnp.sum(values, axis=1, keepdims=True) * (1.0 / width)
            moved = values - center
            spread = jnp.sum(moved * moved, axis=1, keepdims=True) * (1.0 / width)
            normed[pl.ds(at, LN), :] = (moved * lax.rsqrt(spread + 1e-06) * gain[...]).astype(
                jnp.bfloat16
            )
            return carry

        lax.fori_loop(0, CHUNK // LN, norm, 0, unroll=2)
        part = normed[pl.ds(base, CHUNK), :]
        query = jnp.dot(part, wq[...], preferred_element_type=jnp.float32)
        for k in range(CHUNK // QB):
            b = i * (CHUNK // QB) + k
            for g in range(groups):
                turned = rotated(query[k * QB:(k + 1) * QB, g * LANES:(g + 1) * LANES], b) * HEAD ** (-0.5)
                qs[b, pl.ds(2 * g * QB, QB), :] = jnp.where(low_half, turned, 0.0).astype(jnp.bfloat16)
                qs[b, pl.ds((2 * g + 1) * QB, QB), :] = jnp.where(
                    low_half, pltpu.roll(turned, HEAD, 1), 0.0
                ).astype(jnp.bfloat16)
        mixed = jnp.dot(part, wp[...], preferred_element_type=jnp.float32)
        pool[pl.ds(pl.multiple_of(reach + base, 8), CHUNK), :] = mixed.astype(jnp.bfloat16).astype(jnp.float32)

        @pl.when(i == 0)
        def _():
            x_in.wait_recv()
            for copy in wo_crossed:
                copy.start()

        @pl.when(i == 2)
        def _():
            own_copies[2].wait()
            for copy in kv_forward[1:]:
                copy.wait_recv()
            for copy in kv_forward:
                copy.start()
        return carry

    lax.fori_loop(0, chunks, project, 0)

    halo_pool = [
        remote(pool.at[pl.ds(rows, reach)], pool.at[pl.ds(0, reach)], halo_send.at[0], halo_recv.at[0], after, t),
        remote(pool.at[pl.ds(reach, reach)], pool.at[pl.ds(rows + reach, reach)], halo_send.at[1], halo_recv.at[1], before, t),
    ]
    halo_kv = [
        remote(kv.at[pl.ds(rows, WINDOW)], kv.at[pl.ds(0, WINDOW)], halo_send.at[2], halo_recv.at[2], after, t),
        remote(kv.at[pl.ds(WINDOW, WINDOW)], kv.at[pl.ds(rows + WINDOW, WINDOW)], halo_send.at[3], halo_recv.at[3], before, t),
    ]

    for b in [partner] + [zmate(d, partner) for d in hops] + [zmate(d, partner + 2 - 4 * y) for d in range(Z)]:
        remote(kvw.at[b], kvw.at[b], kvf_send.at[0], kv_recv.at[b], partner, t).wait_recv()

    def key_value(j, carry):
        i = jnp.where(j == 0, 0, jnp.where(j == 1, chunks - 1, j - 1))
        base = pl.multiple_of(i * CHUNK, CHUNK)
        both = jnp.dot(
            normed[pl.ds(base, CHUNK), :], kvw[...].reshape(width, LANES), preferred_element_type=jnp.float32
        )
        for k in range(CHUNK // QB):
            piece = both[k * QB:(k + 1) * QB, :]
            turned = rotated(piece, i * (CHUNK // QB) + k)
            kv[pl.ds(pl.multiple_of(WINDOW + base + k * QB, QB), QB), :] = jnp.where(
                low_half, turned, piece
            ).astype(jnp.bfloat16)

        @pl.when(j == 0)
        def _():
            for copy in halo_pool:
                copy.start()

        @pl.when(j == 2)
        def _():
            for copy in halo_kv:
                copy.start()
        return carry

    lax.fori_loop(0, chunks, key_value, 0)

    for copy in halo_pool:
        copy.wait_recv()

    @pl.when(s == 0)
    def _():
        pool[0:reach, :] = jnp.zeros((reach, pool.shape[1]), jnp.float32)

    @pl.when(s == S - 1)
    def _():
        pool[rows + reach:rows + 2 * reach, :] = jnp.zeros((reach, pool.shape[1]), jnp.float32)

    def pooled(b, g):
        cols = slice(g * LANES, (g + 1) * LANES)
        length = QB + 2 * reach
        values = pool[pl.ds(pl.multiple_of(b * QB, QB), length), cols]
        index = (t * (pgroups * LANES) + g * LANES) // POOL_CH
        running = values
        stride = 1
        picked = jnp.zeros((QB, LANES), jnp.float32)
        wide = 0
        for k, span in enumerate(POOL_SPANS):
            running = running + pltpu.roll(running, length - stride, 0)
            stride = span
            shift = reach - span // 2
            sums = (pltpu.roll(running, length - shift, 0) if shift else running)[:QB]
            picked = jnp.where(index == k, sums, picked)
            wide = jnp.where(index == k, span // 2, wide)
        pos = offset + b * QB + lax.broadcasted_iota(jnp.int32, (QB, LANES), 0)
        counted = (jnp.minimum(pos + wide, total_rows) - jnp.maximum(pos - wide, 0)).astype(jnp.float32)
        return ((picked / counted - values[reach:reach + QB]) * scale[:, cols]).astype(jnp.bfloat16)

    def pool_other(i, carry):
        for g in range(pgroups):
            pool_send[pl.ds(pl.multiple_of(i * QB, QB), QB), g * LANES:(g + 1) * LANES] = pooled(cross * hb + i, g)
        return carry

    def pool_own(i, carry):
        for g in range(pgroups):
            joined[T + t, pl.ds(pl.multiple_of(i * QB, QB), QB), g * LANES:(g + 1) * LANES] = pooled(t * hb + i, g)
        return carry

    ex_pool = remote(pool_send, joined.at[T + t], ex_send.at[0], ex_recv.at[0], s, cross)
    ex_att = remote(att_send, joined.at[t], ex_send.at[1], ex_recv.at[1], s, cross)
    lax.fori_loop(0, hb, pool_other, 0)
    lax.fori_loop(0, hb, pool_own, 0)
    ex_pool.start()
    for i in range(len(hops)):
        forward_z(i, 0)

    span = QB + 2 * WINDOW
    row_id = lax.broadcasted_iota(jnp.int32, (QB, span), 0)
    col_id = lax.broadcasted_iota(jnp.int32, (QB, span), 1)

    def attend(b):
        context = kv[pl.ds(pl.multiple_of(b * QB, QB), span), :]
        scores = lax.dot_general(
            qs[b], context, (((1,), (1,)), ((), ())), preferred_element_type=jnp.float32
        )
        start = offset + b * QB
        lowest = jnp.maximum(row_id, WINDOW - start)
        highest_col = jnp.minimum(row_id + 2 * WINDOW, total_rows - 1 - start + WINDOW)
        valid = (col_id >= lowest) & (col_id <= highest_col)
        expos = []
        norms = []
        for h in range(local_heads):
            part = jnp.where(valid, scores[h * QB:(h + 1) * QB], NEG_BIG)
            top = jnp.maximum(jnp.max(part, axis=1, keepdims=True), sink[h])
            expo = jnp.exp(part - top)
            norms.append(1.0 / (jnp.sum(expo, axis=1, keepdims=True) + jnp.exp(sink[h] - top)))
            expos.append(expo.astype(jnp.bfloat16))
        result = jnp.dot(jnp.concatenate(expos, axis=0), context, preferred_element_type=jnp.float32)
        heads = [result[h * QB:(h + 1) * QB] * norms[h] for h in range(local_heads)]
        return [
            jnp.where(low_half, pltpu.roll(heads[2 * g], HEAD, 1), heads[2 * g + 1]).astype(jnp.bfloat16)
            for g in range(groups)
        ]

    def attend_other(i, carry):
        @pl.when(i == hb - 1)
        def _():
            halo_kv[0].wait_recv()
            halo_kv[1].wait_recv()
        b = jnp.where(t == 0, hb + i, hb - 1 - i)
        at = pl.multiple_of((b - cross * hb) * QB, QB)
        for g, value in enumerate(attend(b)):
            att_send[pl.ds(at, QB), g * LANES:(g + 1) * LANES] = value
        return carry

    def attend_own(i, carry):
        b = jnp.where(t == 0, hb - 1 - i, hb + i)
        at = pl.multiple_of((b - t * hb) * QB, QB)
        for g, value in enumerate(attend(b)):
            joined[t, pl.ds(at, QB), g * LANES:(g + 1) * LANES] = value

        @pl.when(i == 0)
        def _():
            ex_att.start()
        return carry

    lax.fori_loop(0, hb, attend_other, 0)
    lax.fori_loop(0, hb, attend_own, 0)
    for i in range(len(hops)):
        forward_z(i, 1)
    for d in range(Z):
        forward_y(d, 0)
    own_copies[3].wait()

    remote(pool_send, joined.at[T + cross], ex_send.at[0], ex_recv.at[0], s, cross).wait_recv()
    remote(att_send, joined.at[cross], ex_send.at[1], ex_recv.at[1], s, cross).wait_recv()
    def out_copy(n):
        return pltpu.make_async_copy(
            out_v.at[n], out.at[:, pl.ds(pl.multiple_of(n * 2 * LANES, 2 * LANES), 2 * LANES)], out_sem.at[n]
        )

    def finish(j, carry):
        over = j // Z
        @pl.when(over == 0)
        def _():
            forward_y(j, 1)
        side = y + over - 2 * y * over
        n = ((z + j) % Z) * 2 + side
        for half in range(T):
            piece = wfull.at[2 * n + 1 - c, half]
            remote(piece, piece, wp_send.at[0, 0], wo_recv.at[2 * n + 1 - c, half], partner, t).wait_recv()
        left = jnp.concatenate([joined[k] for k in range(2 * T)], axis=1)
        right = jnp.concatenate(
            [wfull[2 * n].reshape(left.shape[1], LANES), wfull[2 * n + 1].reshape(left.shape[1], LANES)], axis=1
        )
        out_v[n] = jnp.dot(left, right, preferred_element_type=jnp.float32).astype(jnp.bfloat16)
        out_copy(n).start()
        return carry

    lax.fori_loop(0, S // 2, finish, 0)
    for copy in kv_copies + [x_copy] + kv_forward + wo_own + wo_crossed + halo_pool + halo_kv + [ex_pool, ex_att]:
        copy.wait_send()
    for k in range(2):
        for i in range(len(hops)):
            for copy in z_copies(i, k):
                copy.wait_send()
        for d in range(Z):
            y_copy(d, k).wait_send()
    for n in range(S // 2):
        out_copy(n).wait()


def body(mesh, tokens, norm_gain, w_query, w_key, w_value, w_pool_in, sink_logit, pool_scale, w_out):
    S = lax.axis_size("sp")
    T = lax.axis_size("tp")
    rows, width = tokens.shape
    local_heads = w_query.shape[1] // HEAD
    fits = (
        S % 4 == 0 and S > 4 and T == 2
        and w_out.shape[1] == LANES and w_key.shape[0] == LANES
        and w_query.shape[1] % LANES == 0 and w_pool_in.shape[1] % LANES == 0
        and w_query.shape[1] == w_pool_in.shape[1]
        and local_heads == QH // KVH and rows % (2 * CHUNK) == 0
    )
    if not fits:
        return plain_body(
            tokens, norm_gain, w_query, w_key, w_value, w_pool_in, sink_logit, pool_scale, w_out
        )
    place = lax.axis_index("tp")
    key_head = place * local_heads // (QH // KVH)
    kv_block = jnp.concatenate(
        [
            lax.dynamic_slice_in_dim(w_key, key_head * HEAD, HEAD, 1),
            lax.dynamic_slice_in_dim(w_value, key_head * HEAD, HEAD, 1),
        ],
        axis=1,
    )
    tables = rope_tables(lax.axis_index("sp") * rows, rows)
    blocks = rows // QB
    half = rows // T
    Z = S // 4
    reach = POOL_SPANS[-1] // 2
    wide = w_query.shape[1]
    vmem = pl.BlockSpec(memory_space=pltpu.VMEM)
    smem = pl.BlockSpec(memory_space=pltpu.SMEM)
    hbm = pl.BlockSpec(memory_space=pl.ANY)
    dma = pltpu.SemaphoreType.DMA
    bf = jnp.bfloat16
    return pl.pallas_call(
        functools.partial(mixer_kernel, (S, T)),
        out_shape=jax.ShapeDtypeStruct((half, S * w_out.shape[1]), bf),
        in_specs=[hbm, vmem, hbm, hbm, hbm, smem, vmem, hbm, vmem, vmem, vmem, vmem],
        out_specs=hbm,
        scratch_shapes=[
            pltpu.VMEM((rows, width), bf),
            pltpu.VMEM((rows, width), bf),
            pltpu.VMEM(w_query.shape, bf),
            pltpu.VMEM(w_pool_in.shape, bf),
            pltpu.VMEM((S, LANES, LANES), bf),
            pltpu.VMEM((S, T) + w_out.shape, bf),
            pltpu.VMEM((blocks, local_heads * QB, LANES), bf),
            pltpu.VMEM((rows + 2 * WINDOW, LANES), bf),
            pltpu.VMEM((rows + 2 * reach, wide), jnp.float32),
            pltpu.VMEM((half, wide), bf),
            pltpu.VMEM((half, wide), bf),
            pltpu.VMEM((2 * T, half, wide), bf),
            pltpu.VMEM((S // 2, half, 2 * LANES), bf),
            dma((rows // CHUNK,)),
            dma((4,)),
            dma((S // 2,)),
            dma((S // 2 - 1,)),
            dma((S,)),
            dma((S // 2,)),
            dma(()),
            dma(()),
            dma((T, Z + 1)),
            dma((S, T)),
            dma((T, 2 * (Z - 1))),
            dma((T, Z)),
            dma((4,)),
            dma((4,)),
            dma((2,)),
            dma((2,)),
        ],
        compiler_params=pltpu.CompilerParams(
            collective_id=0, has_side_effects=True, vmem_limit_bytes=62 * 1024 * 1024
        ),
    )(
        tokens, norm_gain[None, :], w_query, kv_block, w_pool_in, sink_logit, pool_scale[None, :], w_out, *tables
    )


def solution(mesh):
    in_specs = (
        P("sp", None),
        P(),
        P(None, "tp"),
        P("sp", None),
        P("sp", None),
        P(None, "tp"),
        P("tp"),
        P("tp"),
        P("tp", "sp"),
    )
    out_specs = P(("sp", "tp"), None)
    return jax.shard_map(functools.partial(body, mesh), mesh=mesh, in_specs=in_specs, out_specs=out_specs, check_vma=False)
```

profile of v0, /device:TPU:9, one launch (start us, length us, event | category | flops | bytes accessed | tf_op | source)
XLA Modules:
  0.0 58.3 jit_solution(9687799489161220409)
XLA Ops:
  0.0 0.1 mul.74
  0.1 0.7 %fusion.1 = (f32[8,128]{1,0:T(8,128)}, f32[8,128]{1,0:T(8,128)}) fusion(f32[128]{0:T(128)S(1)} %compare_select_fusion, f32[128]{0:T(128)S(1)} %mul.74, f32[8]{0:T(128)S(1)} %add_convert_fusion), kind=kLoop, calls=%fused_computation.6 | loop fusion | flops 2048 | bytes 9248 | tf_op jit(solution)/shard_map/mul | solution.py:161
  0.8 0.9 %constant_dynamic-slice_fusion = (bf16[128,64]{1,0:T(8,128)(2,1)S(1)}, bf16[128,64]{1,0:T(8,128)(2,1)S(1)}) fusion(bf16[128,128]{1,0:T(8,128)(2,1)} %param.13, s32[]{:T(128)S(6)} %select_n.32, bf16[128,128]{1,0:T(8,128)(2,1)} %param.12), kind=kLoop, calls=%fused_computation.11 | loop fusion | bytes 65540 | tf_op jit(solution)/shard_map/dynamic_slice | solution.py:558
  1.7 0.7 %pad_maximum_fusion.kv_block = bf16[128,128]{1,0:T(8,128)(2,1)} fusion(bf16[128,64]{1,0:T(8,128)(2,1)S(1)} %get-tuple-element.9, bf16[128,64]{1,0:T(8,128)(2,1)S(1)} %get-tuple-element.10), kind=kLoop, calls=%fused_computation.3 | loop fusion | flops 65536 | bytes 65536 | tf_op jit(solution)/shard_map/concatenate | solution.py:555
  2.4 0.9 %sine_multiply_fusion = (f32[128,128]{1,0:T(8,128)}, f32[128,128]{1,0:T(8,128)}) fusion(f32[128]{0:T(128)S(1)} %compare_select_fusion, f32[128]{0:T(128)S(1)} %mul.74), kind=kLoop, calls=%fused_computation | loop fusion | flops 32768 | bytes 132096 | tf_op jit(solution)/shard_map/mul | solution.py:161
  3.3 51.8 %shard_map.91 = bf16[512,2048]{1,0:T(8,128)(2,1)} custom-call(bf16[1024,2048]{1,0:T(8,128)(2,1)} %tokens.1, f32[1,2048]{1,0:T(1,128)} %bitcast.2, bf16[2048,256]{1,0:T(8,128)(2,1)} %w_query.1, bf16[128,128]{1,0:T(8,128)(2,1)} %pad_maximum_fusion.kv_block, bf16[2048,256]{1,0:T(8,128)(2,1)} %w_pool.1, f32[4]{0:T(128)} %sink.1, f32[1,256]{1,0:T(1,128)} %bitcast.3, ...), custom_call_target="tpu_custom_call" | custom-call | tf_op jit(solution)/shard_map/pallas_call | solution.py:573
  55.2 3.2 %copy.11 = bf16[512,2048]{1,0:T(8,128)(2,1)} copy(bf16[512,2048]{1,0:T(8,128)(2,1)} %shard_map.91) | data formatting | bytes 4194304
  (4 shorter events, 0.0 us)
where the time goes:
time: 58.6 us; the launch traced here: 58.3 us
  Pallas kernels  51.8 us (88%)
  local copies, waits for them, and re-layouts  4.11 us (7%)
  other arithmetic  2.35 us (4%)
    pallas_call x1, Pallas kernels, body(): pl.pallas_call(functools.partial(mixer_kernel, (S, T)), out_shape=jax.Sha...  51.8 us
    unnamed x1, local copies, waits for them, and re-layouts  3.16 us

commit v1 on v0

--- a/solution.py
+++ b/solution.py
@@ -2,6 +2,7 @@
 
 import jax
 import jax.numpy as jnp
+import numpy as np
 from jax import lax
 from jax.experimental import pallas as pl
 from jax.experimental.pallas import tpu as pltpu
@@ -148,25 +149,27 @@
 
 LANES = 128
 CHUNK = 256
+VMEM_LIMIT = 60 * 1024 * 1024
 MESH = pl.DeviceIdType.MESH
 
 
-def rope_tables(offset, rows):
+def rope_tables(rows_total):
     half = HEAD // 2
-    inverse = 10000.0 ** (-jnp.arange(half, dtype=jnp.float32) / half)
-    inverse = jnp.tile(inverse, LANES // half)[None, :]
-    sign = jnp.where(jnp.arange(LANES) % HEAD < half, -1.0, 1.0)[None, :]
-    inner = jnp.arange(QB, dtype=jnp.float32)[:, None] * inverse
-    starts = (offset + QB * jnp.arange(rows // QB)).astype(jnp.float32)[:, None] * inverse
-    return jnp.cos(inner), jnp.sin(inner) * sign, jnp.cos(starts), jnp.sin(starts) * sign
+    inverse = np.tile(10000.0 ** (-np.arange(half, dtype=np.float64) / half), LANES // half)[None, :]
+    sign = np.where(np.arange(LANES) % HEAD < half, -1.0, 1.0)[None, :]
+    inner = np.arange(QB, dtype=np.float64)[:, None] * inverse
+    starts = (QB * np.arange(rows_total // QB, dtype=np.float64))[:, None] * inverse
+    tables = (np.cos(inner), np.sin(inner) * sign, np.cos(starts), np.sin(starts) * sign)
+    return [jnp.asarray(table.astype(np.float32)) for table in tables]
 
 
 def mixer_kernel(
-    places, tokens, gain, w_query, kv_block, w_pool, sink, scale, w_out, cos_in, sin_in, cos_at, sin_at,
+    places, tokens, gain, w_query, w_key, w_value, w_pool, sink, scale, w_out, cos_in, sin_in, cos_all, sin_all,
     out,
-    tok, normed, wq, wp, kvw, wfull, qs, kv, pool, pool_send, att_send, joined, out_v,
-    tok_sem, own_sem, out_sem, kv_send, kv_recv, kvf_send, wx_send, wx_recv, wo_send, wo_recv,
-    wf_send, wp_send, halo_send, halo_recv, ex_send, ex_recv,
+    tok, normed, wq, wp, kv_in, kvw, wfull, qs, kv, pool, pool_send, att_send, joined, acc, cos_at, sin_at,
+    tok_sem, own_sem, kv_recv, kz_send, ko_send, kf_send, ky_send,
+    wo_recv, wz_send, wo_send, wx_send, wd_send, w00_send, w10_send, w01_send, w11_send,
+    halo_send, halo_recv, exp_send, exp_recv, exa_send, exa_recv,
 ):
     S, T = places
     Z = S // 4
@@ -186,16 +189,12 @@
     c = s % 2
     y = (s // 2) % 2
     z = s // 4
-    quad = s % 4
     partner = s + 1 - 2 * c
     yflip = s + 2 - 4 * y
     after = (s + 1) % S
     before = (s + S - 1) % S
     cross = 1 - t
-    hops = sorted(range(1, Z), key=lambda d: (min(d, Z - d), d))
-
-    def zmate(d, base):
-        return ((z + d) % Z) * 4 + base % 4
+    far = [d for k in range(1, Z) for d in (k, -k)]
 
     def remote(a, b, send, recv, to_s, to_t):
         return pltpu.make_async_remote_copy(
@@ -203,87 +202,167 @@
             device_id={"sp": to_s, "tp": to_t}, device_id_type=MESH,
         )
 
-    same_core = [zmate(d, s) for d in hops] + [zmate(d, yflip) for d in range(Z)]
-
     tok_copies = [
         pltpu.make_async_copy(
             tokens.at[pl.ds(i * CHUNK, CHUNK)], tok.at[pl.ds(i * CHUNK, CHUNK)], tok_sem.at[i]
         )
         for i in range(chunks)
     ]
+    own_copies = [
+        pltpu.make_async_copy(w_key, kv_in.at[0], own_sem.at[0]),
+        pltpu.make_async_copy(w_value, kv_in.at[1], own_sem.at[1]),
+        pltpu.make_async_copy(w_out, wfull.at[s, t], own_sem.at[2]),
+        pltpu.make_async_copy(w_query, wq, own_sem.at[3]),
+        pltpu.make_async_copy(w_pool, wp, own_sem.at[4]),
+        pltpu.make_async_copy(cos_all.at[pl.ds(pl.multiple_of(s * blocks, blocks), blocks)], cos_at, own_sem.at[5]),
+        pltpu.make_async_copy(sin_all.at[pl.ds(pl.multiple_of(s * blocks, blocks), blocks)], sin_at, own_sem.at[6]),
+    ]
+    barrier = pltpu.get_barrier_semaphore()
+    greet = [(((z + d) % Z) * 4 + s % 4, t) for d in range(1, Z)]
+    greet += [(yflip, t), (after, t), (before, t), (s, cross)]
+    for to_s, to_t in greet:
+        pl.semaphore_signal(barrier, inc=1, device_id={"sp": to_s, "tp": to_t}, device_id_type=MESH)
+    for copy in own_copies[:3]:
+        copy.start()
     tok_copies[0].start()
-    own_copies = [
-        pltpu.make_async_copy(w_query, wq, own_sem.at[0]),
-        pltpu.make_async_copy(w_pool, wp, own_sem.at[1]),
-        pltpu.make_async_copy(kv_block, kvw.at[s], own_sem.at[2]),
-        pltpu.make_async_copy(w_out, wfull.at[s, t], own_sem.at[3]),
-    ]
-    for copy in own_copies:
+    for copy in own_copies[3:]:
         copy.start()
     for copy in tok_copies[1:]:
         copy.start()
 
-    barrier = pltpu.get_barrier_semaphore()
-    greet = [(b, t) for b in same_core + [after, before]] + [(s, cross)]
-    for to_s, to_t in greet:
-        pl.semaphore_signal(barrier, inc=1, device_id={"sp": to_s, "tp": to_t}, device_id_type=MESH)
-    pl.semaphore_wait(barrier, len(greet))
-
-    kv_copies = [
-        remote(kv_block, kvw.at[s], kv_send.at[i], kv_recv.at[s], b, t)
-        for i, b in enumerate(same_core)
-    ]
-    for copy in kv_copies:
-        copy.start()
-    x_copy = remote(w_out, wfull.at[s, t], wx_send, wx_recv, s, cross)
-    x_copy.start()
-    x_in = remote(w_out, wfull.at[s, cross], wx_send, wx_recv, s, cross)
-
-    kv_forward = [
-        remote(kvw.at[b], kvw.at[b], kvf_send.at[i], kv_recv.at[b], partner, t)
-        for i, b in enumerate([s] + same_core)
-    ]
-    wo_to = [zmate(d, s) for d in hops] + [yflip, partner]
-    wo_own = [
-        remote(w_out, wfull.at[s, t], wo_send.at[0, i], wo_recv.at[s, t], b, t)
-        for i, b in enumerate(wo_to)
-    ]
-    wo_crossed = [
-        remote(wfull.at[s, cross], wfull.at[s, cross], wo_send.at[1, i], wo_recv.at[s, cross], b, t)
-        for i, b in enumerate(wo_to)
-    ]
-    for copy in wo_own:
-        copy.start()
-
-    def z_copies(i, k):
-        b = zmate(hops[i], s)
-        half = cross if k else t
-        piece = wfull.at[b, half]
-        return [
-            remote(piece, piece, wf_send.at[k, 2 * i + j], wo_recv.at[b, half], to, t)
-            for j, to in enumerate([yflip, partner])
-        ]
-
-    def y_copy(d, k):
-        b = zmate(d, yflip)
-        half = cross if k else t
-        piece = wfull.at[b, half]
-        return remote(piece, piece, wp_send.at[k, d], wo_recv.at[b, half], partner, t)
-
-    def forward_z(i, k):
-        copies = z_copies(i, k)
-        copies[0].wait_recv()
-        for copy in copies:
-            copy.start()
-
-    def forward_y(d, k):
-        copy = y_copy(d, k)
-        copy.wait_recv()
-        copy.start()
-
     lane = lax.broadcasted_iota(jnp.int32, (QB, LANES), 1)
     low_half = lane < HEAD
     first_half = lane % HEAD < HEAD // 2
+
+    own_copies[0].wait()
+    own_copies[1].wait()
+    key_head = t * local_heads // (QH // KVH)
+    key_in = kv_in[0].astype(jnp.float32)
+    value_in = kv_in[1].astype(jnp.float32)
+    key_cols = jnp.where(key_head == 0, key_in, pltpu.roll(key_in, HEAD, 1))
+    value_cols = jnp.where(key_head == 0, pltpu.roll(value_in, HEAD, 1), value_in)
+    kvw[s] = jnp.where(low_half, key_cols, value_cols).astype(jnp.bfloat16)
+    own_copies[2].wait()
+    pl.semaphore_wait(barrier, len(greet))
+
+    pending = []
+
+    def go(cond, make):
+        pending.append((cond, make))
+        if cond is None:
+            make().start()
+        else:
+            @pl.when(cond)
+            def _():
+                make().start()
+
+    def later(cond, make):
+        pending.append((cond, make))
+
+    def here(d):
+        return (z + d >= 0) & (z + d < Z)
+
+    def piece_kv(b):
+        return kvw.at[b]
+
+    def piece_wo(b, half):
+        return wfull.at[b, half]
+
+    def kv_copy(b, send, to):
+        return lambda: remote(kvw.at[b], kvw.at[b], send, kv_recv.at[b], to, t)
+
+    def wo_copy(b, half, send, to_s, to_t):
+        return lambda: remote(wfull.at[b, half], wfull.at[b, half], send, wo_recv.at[b, half], to_s, to_t)
+
+    hop = [1, -1, 2, -2]
+
+    def at_z(d):
+        return s + 4 * d
+
+    def at_yz(d):
+        return yflip + 4 * d
+
+    def reach_index(d):
+        return far.index(d)
+
+    def start_all(items):
+        for cond, make in items:
+            if cond is None:
+                make().start()
+            else:
+                @pl.when(cond)
+                def _(make=make):
+                    make().start()
+
+    def event(cond, arrival, items):
+        pending.extend([(cond if k is None else (k if cond is None else cond & k), m) for k, m in items])
+
+        def act():
+            def inner():
+                if arrival is not None:
+                    arrival().wait_recv()
+                start_all(items)
+            if cond is None:
+                inner()
+            else:
+                pl.when(cond)(inner)
+        return act
+
+    def onward(d):
+        step = -1 if d > 0 else 1
+        return step, here(step)
+
+    ev = {}
+    ev["kv_own"] = event(None, None,
+        [(here(h), kv_copy(s, kz_send.at[i], at_z(h))) for i, h in enumerate(hop) if abs(h) < Z]
+        + [(None, kv_copy(s, ko_send.at[0], yflip)), (None, kv_copy(s, ko_send.at[1], partner))])
+    for i, d in enumerate(far):
+        step, fine = onward(d)
+        items = [(None, kv_copy(at_z(d), kf_send.at[i, 0], yflip)), (None, kv_copy(at_z(d), kf_send.at[i, 1], partner))]
+        if 2 <= abs(d) < Z - 1:
+            items = [(fine, kv_copy(at_z(d), kf_send.at[i, 2], at_z(step)))] + items
+        ev["kv", d] = event(here(d), kv_copy(at_z(d), kf_send.at[i, 0], yflip), items)
+    for i, d in enumerate([0] + far):
+        ev["kvy", d] = event(None if d == 0 else here(d), kv_copy(at_yz(d), ky_send.at[i], partner),
+            [(None, kv_copy(at_yz(d), ky_send.at[i], partner))])
+
+    ev["wo_own"] = event(None, None,
+        [(None, wo_copy(s, t, wo_send.at[0], s, cross)), (None, wo_copy(s, t, wo_send.at[1], yflip, t))]
+        + [(here(h), wo_copy(s, t, wz_send.at[i], at_z(h), t)) for i, h in enumerate(hop) if abs(h) < Z]
+        + [(None, wo_copy(s, t, wo_send.at[2], partner, t))])
+    ev["wo_x"] = event(None, wo_copy(s, cross, wx_send.at[0], yflip, t),
+        [(None, wo_copy(s, cross, wx_send.at[0], yflip, t)), (None, wo_copy(s, cross, wx_send.at[1], partner, t))])
+    ev["wo_d"] = event(None, wo_copy(yflip, cross, wd_send.at[4], partner, t),
+        [(here(h), wo_copy(yflip, cross, wd_send.at[i], at_z(h), t)) for i, h in enumerate(hop) if abs(h) < Z]
+        + [(None, wo_copy(yflip, cross, wd_send.at[4], partner, t))])
+    for i, d in enumerate(far):
+        step, fine = onward(d)
+        b = at_z(d)
+        items = [(None, wo_copy(b, t, w00_send.at[i, 0], s, cross)), (None, wo_copy(b, t, w00_send.at[i, 1], yflip, t)),
+                 (None, wo_copy(b, t, w00_send.at[i, 2], partner, t))]
+        if 2 <= abs(d) < Z - 1:
+            items = [(fine, wo_copy(b, t, w00_send.at[i, 3], at_z(step), t))] + items
+        ev["w00", d] = event(here(d), wo_copy(b, t, w00_send.at[i, 0], s, cross), items)
+        ev["w10", d] = event(here(d), wo_copy(b, cross, w10_send.at[i], partner, t),
+            [(None, wo_copy(b, cross, w10_send.at[i], partner, t))])
+        b = at_yz(d)
+        items = [(None, wo_copy(b, cross, w11_send.at[i, 0], partner, t))]
+        if 2 <= abs(d) < Z - 1:
+            items = [(fine, wo_copy(b, cross, w11_send.at[i, 1], at_z(step), t))] + items
+        ev["w11", d] = event(here(d), wo_copy(b, cross, w11_send.at[i, 0], partner, t), items)
+    for i, d in enumerate([0] + far):
+        b = at_yz(d)
+        ev["w01", d] = event(None if d == 0 else here(d), wo_copy(b, t, w01_send.at[i], partner, t),
+            [(None, wo_copy(b, t, w01_send.at[i], partner, t))])
+
+    def poll(kind, *distances):
+        for k in distances:
+            for d in ((k, -k) if k else (0,)):
+                if abs(d) < Z:
+                    ev[kind, d]()
+
+    ev["kv_own"]()
+    ev["wo_own"]()
 
     def rotated(values, b):
         ca = cos_at[pl.ds(b, 1), :]
@@ -299,8 +378,8 @@
         )
         return values * cosine + swapped * sine
 
-    own_copies[0].wait()
-    own_copies[1].wait()
+    for copy in own_copies[3:]:
+        copy.wait()
     LN = 32
 
     def project(i, carry):
@@ -334,34 +413,71 @@
         mixed = jnp.dot(part, wp[...], preferred_element_type=jnp.float32)
         pool[pl.ds(pl.multiple_of(reach + base, 8), CHUNK), :] = mixed.astype(jnp.bfloat16).astype(jnp.float32)
 
-        @pl.when(i == 0)
-        def _():
-            x_in.wait_recv()
-            for copy in wo_crossed:
-                copy.start()
+
+        @pl.when(i == 1)
+        def _():
+            poll("kv", 1)
 
         @pl.when(i == 2)
         def _():
-            own_copies[2].wait()
-            for copy in kv_forward[1:]:
-                copy.wait_recv()
-            for copy in kv_forward:
-                copy.start()
+            poll("kv", 2)
+            poll("kvy", 0)
+            ev["wo_x"]()
+
+        @pl.when(i == 3)
+        def _():
+            poll("kv", *range(3, Z))
+            poll("kvy", 1)
+            poll("w00", 1)
         return carry
 
     lax.fori_loop(0, chunks, project, 0)
 
+    inner = s < S - 1
+    outer = s > 0
     halo_pool = [
-        remote(pool.at[pl.ds(rows, reach)], pool.at[pl.ds(0, reach)], halo_send.at[0], halo_recv.at[0], after, t),
-        remote(pool.at[pl.ds(reach, reach)], pool.at[pl.ds(rows + reach, reach)], halo_send.at[1], halo_recv.at[1], before, t),
+        (inner, lambda: remote(pool.at[pl.ds(rows, reach)], pool.at[pl.ds(0, reach)], halo_send.at[0], halo_recv.at[0], after, t)),
+        (outer, lambda: remote(pool.at[pl.ds(reach, reach)], pool.at[pl.ds(rows + reach, reach)], halo_send.at[1], halo_recv.at[1], before, t)),
     ]
     halo_kv = [
-        remote(kv.at[pl.ds(rows, WINDOW)], kv.at[pl.ds(0, WINDOW)], halo_send.at[2], halo_recv.at[2], after, t),
-        remote(kv.at[pl.ds(WINDOW, WINDOW)], kv.at[pl.ds(rows + WINDOW, WINDOW)], halo_send.at[3], halo_recv.at[3], before, t),
+        (inner, lambda: remote(kv.at[pl.ds(rows, WINDOW)], kv.at[pl.ds(0, WINDOW)], halo_send.at[2], halo_recv.at[2], after, t)),
+        (outer, lambda: remote(kv.at[pl.ds(WINDOW, WINDOW)], kv.at[pl.ds(rows + WINDOW, WINDOW)], halo_send.at[3], halo_recv.at[3], before, t)),
     ]
-
-    for b in [partner] + [zmate(d, partner) for d in hops] + [zmate(d, partner + 2 - 4 * y) for d in range(Z)]:
-        remote(kvw.at[b], kvw.at[b], kvf_send.at[0], kv_recv.at[b], partner, t).wait_recv()
+    pending.extend(halo_pool + halo_kv)
+
+    def halo_wait(pair):
+        @pl.when(outer)
+        def _():
+            pair[0][1]().wait_recv()
+
+        @pl.when(inner)
+        def _():
+            pair[1][1]().wait_recv()
+
+    start_all(halo_pool)
+
+    @pl.when(s == 0)
+    def _():
+        pool[0:reach, :] = jnp.zeros((reach, pool.shape[1]), jnp.float32)
+        kv[0:WINDOW, :] = jnp.zeros((WINDOW, LANES), jnp.bfloat16)
+
+    @pl.when(s == S - 1)
+    def _():
+        pool[rows + reach:rows + 2 * reach, :] = jnp.zeros((reach, pool.shape[1]), jnp.float32)
+        kv[rows + WINDOW:rows + 2 * WINDOW, :] = jnp.zeros((WINDOW, LANES), jnp.bfloat16)
+
+    poll("kvy", *range(2, Z))
+    own_core = [s] + [at_z(d) for d in far] + [yflip] + [at_yz(d) for d in far]
+    arrives = [(None, partner), (None, yflip + partner - s)]
+    arrives += [(here(d), partner + 4 * d) for d in far] + [(here(d), yflip + partner - s + 4 * d) for d in far]
+    for cond, b in arrives:
+        make = kv_copy(b, ko_send.at[1], partner)
+        if cond is None:
+            make().wait_recv()
+        else:
+            @pl.when(cond)
+            def _(make=make):
+                make().wait_recv()
 
     def key_value(j, carry):
         i = jnp.where(j == 0, 0, jnp.where(j == 1, chunks - 1, j - 1))
@@ -378,27 +494,16 @@
 
         @pl.when(j == 0)
         def _():
-            for copy in halo_pool:
-                copy.start()
+            ev["wo_d"]()
 
         @pl.when(j == 2)
         def _():
-            for copy in halo_kv:
-                copy.start()
+            start_all(halo_kv)
+            poll("w00", 2)
         return carry
 
     lax.fori_loop(0, chunks, key_value, 0)
-
-    for copy in halo_pool:
-        copy.wait_recv()
-
-    @pl.when(s == 0)
-    def _():
-        pool[0:reach, :] = jnp.zeros((reach, pool.shape[1]), jnp.float32)
-
-    @pl.when(s == S - 1)
-    def _():
-        pool[rows + reach:rows + 2 * reach, :] = jnp.zeros((reach, pool.shape[1]), jnp.float32)
+    halo_wait(halo_pool)
 
     def pooled(b, g):
         cols = slice(g * LANES, (g + 1) * LANES)
@@ -430,13 +535,20 @@
             joined[T + t, pl.ds(pl.multiple_of(i * QB, QB), QB), g * LANES:(g + 1) * LANES] = pooled(t * hb + i, g)
         return carry
 
-    ex_pool = remote(pool_send, joined.at[T + t], ex_send.at[0], ex_recv.at[0], s, cross)
-    ex_att = remote(att_send, joined.at[t], ex_send.at[1], ex_recv.at[1], s, cross)
+
+    ex_pool = (None, lambda: remote(pool_send, joined.at[T + t], exp_send.at[0], exp_recv.at[0], s, cross))
+    pending.append(ex_pool)
+
+    def ex_att(n):
+        at = pl.ds(pl.multiple_of(n * QB, QB), QB)
+        return remote(att_send.at[at], joined.at[t, at], exa_send.at[n], exa_recv.at[n], s, cross)
+
     lax.fori_loop(0, hb, pool_other, 0)
+    ex_pool[1]().start()
+    poll("w00", *range(3, Z))
     lax.fori_loop(0, hb, pool_own, 0)
-    ex_pool.start()
-    for i in range(len(hops)):
-        forward_z(i, 0)
+    poll("w10", 1)
+    poll("w01", 0, 1)
 
     span = QB + 2 * WINDOW
     row_id = lax.broadcasted_iota(jnp.int32, (QB, span), 0)
@@ -466,15 +578,21 @@
             for g in range(groups)
         ]
 
+
     def attend_other(i, carry):
         @pl.when(i == hb - 1)
         def _():
-            halo_kv[0].wait_recv()
-            halo_kv[1].wait_recv()
+            halo_wait(halo_kv)
         b = jnp.where(t == 0, hb + i, hb - 1 - i)
-        at = pl.multiple_of((b - cross * hb) * QB, QB)
+        n = b - cross * hb
+        at = pl.multiple_of(n * QB, QB)
         for g, value in enumerate(attend(b)):
             att_send[pl.ds(at, QB), g * LANES:(g + 1) * LANES] = value
+        ex_att(n).start()
+
+        @pl.when(i == 1)
+        def _():
+            poll("w11", 1)
         return carry
 
     def attend_own(i, carry):
@@ -485,53 +603,65 @@
 
         @pl.when(i == 0)
         def _():
-            ex_att.start()
+            poll("w10", 2)
+            poll("w01", 2)
+
+        @pl.when(i == 2)
+        def _():
+            poll("w11", 2)
         return carry
 
     lax.fori_loop(0, hb, attend_other, 0)
     lax.fori_loop(0, hb, attend_own, 0)
-    for i in range(len(hops)):
-        forward_z(i, 1)
-    for d in range(Z):
-        forward_y(d, 0)
-    own_copies[3].wait()
-
-    remote(pool_send, joined.at[T + cross], ex_send.at[0], ex_recv.at[0], s, cross).wait_recv()
-    remote(att_send, joined.at[cross], ex_send.at[1], ex_recv.at[1], s, cross).wait_recv()
-    def out_copy(n):
-        return pltpu.make_async_copy(
-            out_v.at[n], out.at[:, pl.ds(pl.multiple_of(n * 2 * LANES, 2 * LANES), 2 * LANES)], out_sem.at[n]
-        )
-
-    def finish(j, carry):
+    poll("w10", *range(3, Z))
+    poll("w01", *range(3, Z))
+
+    remote(pool_send, joined.at[T + cross], exp_send.at[0], exp_recv.at[0], s, cross).wait_recv()
+    wide = joined.shape[2]
+
+    def columns(n, half, start, count):
+        at = pl.ds(pl.multiple_of(start, wide), count)
+        return jnp.concatenate([wfull[2 * n, half, at, :], wfull[2 * n + 1, half, at, :]], axis=1)
+
+    def most(j, carry):
         over = j // Z
-        @pl.when(over == 0)
-        def _():
-            forward_y(j, 1)
+        @pl.when(j == 2)
+        def _():
+            poll("w11", *range(3, Z))
         side = y + over - 2 * y * over
-        n = ((z + j) % Z) * 2 + side
+        k = j % Z
+        zz = jnp.where(z < Z // 2, (z + k) % Z, (z + Z - k) % Z)
+        n = zz * 2 + side
         for half in range(T):
             piece = wfull.at[2 * n + 1 - c, half]
-            remote(piece, piece, wp_send.at[0, 0], wo_recv.at[2 * n + 1 - c, half], partner, t).wait_recv()
-        left = jnp.concatenate([joined[k] for k in range(2 * T)], axis=1)
-        right = jnp.concatenate(
-            [wfull[2 * n].reshape(left.shape[1], LANES), wfull[2 * n + 1].reshape(left.shape[1], LANES)], axis=1
-        )
-        out_v[n] = jnp.dot(left, right, preferred_element_type=jnp.float32).astype(jnp.bfloat16)
-        out_copy(n).start()
+            remote(piece, piece, wo_send.at[2], wo_recv.at[2 * n + 1 - c, half], partner, t).wait_recv()
+        left = jnp.concatenate([joined[t]] + [joined[T + k] for k in range(T)], axis=1)
+        right = jnp.concatenate([columns(n, 0, t * wide, wide), columns(n, 1, 0, T * wide)], axis=0)
+        acc[n] = jnp.dot(left, right, preferred_element_type=jnp.float32)
         return carry
 
-    lax.fori_loop(0, S // 2, finish, 0)
-    for copy in kv_copies + [x_copy] + kv_forward + wo_own + wo_crossed + halo_pool + halo_kv + [ex_pool, ex_att]:
-        copy.wait_send()
-    for k in range(2):
-        for i in range(len(hops)):
-            for copy in z_copies(i, k):
-                copy.wait_send()
-        for d in range(Z):
-            y_copy(d, k).wait_send()
-    for n in range(S // 2):
-        out_copy(n).wait()
+    lax.fori_loop(0, S // 2, most, 0)
+    for n in range(hb):
+        at = pl.ds(n * QB, QB)
+        remote(att_send.at[at], joined.at[cross, at], exa_send.at[n], exa_recv.at[n], s, cross).wait_recv()
+
+    def last(n, carry):
+        total = acc[n] + jnp.dot(
+            joined[cross], columns(n, 0, cross * wide, wide), preferred_element_type=jnp.float32
+        )
+        out[:, pl.ds(pl.multiple_of(n * 2 * LANES, 2 * LANES), 2 * LANES)] = total.astype(jnp.bfloat16)
+        return carry
+
+    lax.fori_loop(0, S // 2, last, 0)
+    for cond, make in pending:
+        if cond is None:
+            make().wait_send()
+        else:
+            @pl.when(cond)
+            def _(make=make):
+                make().wait_send()
+    for n in range(hb):
+        ex_att(n).wait_send()
 
 
 def body(mesh, tokens, norm_gain, w_query, w_key, w_value, w_pool_in, sink_logit, pool_scale, w_out):
@@ -541,7 +671,7 @@
     local_heads = w_query.shape[1] // HEAD
     fits = (
         S % 4 == 0 and S > 4 and T == 2
-        and w_out.shape[1] == LANES and w_key.shape[0] == LANES
+        and w_out.shape[1] == LANES and w_key.shape == (LANES, LANES) and w_value.shape == w_key.shape
         and w_query.shape[1] % LANES == 0 and w_pool_in.shape[1] % LANES == 0
         and w_query.shape[1] == w_pool_in.shape[1]
         and local_heads == QH // KVH and rows % (2 * CHUNK) == 0
@@ -550,36 +680,29 @@
         return plain_body(
             tokens, norm_gain, w_query, w_key, w_value, w_pool_in, sink_logit, pool_scale, w_out
         )
-    place = lax.axis_index("tp")
-    key_head = place * local_heads // (QH // KVH)
-    kv_block = jnp.concatenate(
-        [
-            lax.dynamic_slice_in_dim(w_key, key_head * HEAD, HEAD, 1),
-            lax.dynamic_slice_in_dim(w_value, key_head * HEAD, HEAD, 1),
-        ],
-        axis=1,
-    )
-    tables = rope_tables(lax.axis_index("sp") * rows, rows)
+    tables = rope_tables(S * rows)
     blocks = rows // QB
     half = rows // T
     Z = S // 4
+    F = 2 * (Z - 1)
     reach = POOL_SPANS[-1] // 2
     wide = w_query.shape[1]
     vmem = pl.BlockSpec(memory_space=pltpu.VMEM)
     smem = pl.BlockSpec(memory_space=pltpu.SMEM)
-    hbm = pl.BlockSpec(memory_space=pl.ANY)
+    hbm = pl.BlockSpec(memory_space=pltpu.HBM)
     dma = pltpu.SemaphoreType.DMA
     bf = jnp.bfloat16
     return pl.pallas_call(
         functools.partial(mixer_kernel, (S, T)),
-        out_shape=jax.ShapeDtypeStruct((half, S * w_out.shape[1]), bf),
-        in_specs=[hbm, vmem, hbm, hbm, hbm, smem, vmem, hbm, vmem, vmem, vmem, vmem],
-        out_specs=hbm,
+        out_shape=pltpu.VMEM((half, S * w_out.shape[1]), bf),
+        in_specs=[hbm, vmem, hbm, hbm, hbm, hbm, smem, vmem, hbm, vmem, vmem, hbm, hbm],
+        out_specs=vmem,
         scratch_shapes=[
             pltpu.VMEM((rows, width), bf),
             pltpu.VMEM((rows, width), bf),
             pltpu.VMEM(w_query.shape, bf),
             pltpu.VMEM(w_pool_in.shape, bf),
+            pltpu.VMEM((2,) + w_key.shape, bf),
             pltpu.VMEM((S, LANES, LANES), bf),
             pltpu.VMEM((S, T) + w_out.shape, bf),
             pltpu.VMEM((blocks, local_heads * QB, LANES), bf),
@@ -588,29 +711,37 @@
             pltpu.VMEM((half, wide), bf),
             pltpu.VMEM((half, wide), bf),
             pltpu.VMEM((2 * T, half, wide), bf),
-            pltpu.VMEM((S // 2, half, 2 * LANES), bf),
+            pltpu.VMEM((S // 2, half, 2 * LANES), jnp.float32),
+            pltpu.VMEM((blocks, LANES), jnp.float32),
+            pltpu.VMEM((blocks, LANES), jnp.float32),
             dma((rows // CHUNK,)),
+            dma((7,)),
+            dma((S,)),
             dma((4,)),
-            dma((S // 2,)),
-            dma((S // 2 - 1,)),
-            dma((S,)),
-            dma((S // 2,)),
-            dma(()),
-            dma(()),
-            dma((T, Z + 1)),
+            dma((2,)),
+            dma((F, 3)),
+            dma((F + 1,)),
             dma((S, T)),
-            dma((T, 2 * (Z - 1))),
-            dma((T, Z)),
+            dma((4,)),
+            dma((3,)),
+            dma((2,)),
+            dma((5,)),
+            dma((F, 4)),
+            dma((F,)),
+            dma((F + 1,)),
+            dma((F, 2)),
             dma((4,)),
             dma((4,)),
-            dma((2,)),
-            dma((2,)),
+            dma((1,)),
+            dma((1,)),
+            dma((blocks // 2,)),
+            dma((blocks // 2,)),
         ],
         compiler_params=pltpu.CompilerParams(
-            collective_id=0, has_side_effects=True, vmem_limit_bytes=62 * 1024 * 1024
+            collective_id=0, has_side_effects=True, vmem_limit_bytes=VMEM_LIMIT
         ),
     )(
-        tokens, norm_gain[None, :], w_query, kv_block, w_pool_in, sink_logit, pool_scale[None, :], w_out, *tables
+        tokens, norm_gain[None, :], w_query, w_key, w_value, w_pool_in, sink_logit, pool_scale[None, :], w_out, *tables
     )
 
 

time: 58.6 us -> 45.4 us (0.77)
  the two profiles are of different devices: /device:TPU:9 before, /device:TPU:0 now
where the time goes in v1:
time: 45.4 us; the launch traced here: 45.2 us
  Pallas kernels  43.9 us (97%)
  local copies, waits for them, and re-layouts  1.32 us (3%)
    pallas_call x1, Pallas kernels, body(): pl.pallas_call(functools.partial(mixer_kernel, (S, T)), out_shape=pltpu.V...  43.9 us
    unnamed x1, local copies, waits for them, and re-layouts  1.32 us

profile of v1, /device:TPU:0, one launch (start us, length us, event | category | flops | bytes accessed | tf_op | source)
XLA Modules:
  0.0 45.2 jit_solution(12351677723040598494)
XLA Ops:
  0.0 43.9 %shard_map.127 = bf16[512,2048]{1,0:T(8,128)(2,1)S(1)} custom-call(bf16[1024,2048]{1,0:T(8,128)(2,1)} %tokens.1, f32[1,2048]{1,0:T(1,128)} %bitcast.2, bf16[2048,256]{1,0:T(8,128)(2,1)} %w_query.1, bf16[128,128]{1,0:T(8,128)(2,1)} %w_key.1, bf16[128,128]{1,0:T(8,128)(2,1)} %w_value.1, bf16[2048,256]{1,0:T(8,128)(2,1)} %w_pool.1, f32[4]{0:T(128)} %sink.1, ...), custom_call_target="tpu_custom_call" | custom-call | tf_op jit(solution)/shard_map/pallas_call | solution.py:695
  43.9 1.3 %copy.15 = bf16[512,2048]{1,0:T(8,128)(2,1)} copy(bf16[512,2048]{1,0:T(8,128)(2,1)S(1)} %shard_map.127) | data formatting | bytes 4194304

commit v2 on v1

--- a/solution.py
+++ b/solution.py
@@ -166,7 +166,7 @@
 def mixer_kernel(
     places, tokens, gain, w_query, w_key, w_value, w_pool, sink, scale, w_out, cos_in, sin_in, cos_all, sin_all,
     out,
-    tok, normed, wq, wp, kv_in, kvw, wfull, qs, kv, pool, pool_send, att_send, joined, acc, cos_at, sin_at,
+    gain_v, scale_v, sink_v, cos_v, sin_v, tok, wq, wp, wqp, scale_at, shift_at, kv_in, kvw, wfull, qs, kv, pool, pool_send, att_send, joined, acc, cos_at, sin_at,
     tok_sem, own_sem, kv_recv, kz_send, ko_send, kf_send, ky_send,
     wo_recv, wz_send, wo_send, wx_send, wd_send, w00_send, w10_send, w01_send, w11_send,
     halo_send, halo_recv, exp_send, exp_recv, exa_send, exa_recv,
@@ -202,13 +202,15 @@
             device_id={"sp": to_s, "tp": to_t}, device_id_type=MESH,
         )
 
-    tok_copies = [
-        pltpu.make_async_copy(
-            tokens.at[pl.ds(i * CHUNK, CHUNK)], tok.at[pl.ds(i * CHUNK, CHUNK)], tok_sem.at[i]
-        )
-        for i in range(chunks)
-    ]
+    def chunk_at(i):
+        return pl.multiple_of(jnp.where(t == 0, chunks - 1 - i, i) * CHUNK, CHUNK)
+
+    def tok_copy(i):
+        at = pl.ds(chunk_at(i), CHUNK)
+        return pltpu.make_async_copy(tokens.at[at], tok.at[at], tok_sem.at[i])
+
     own_copies = [
+        pltpu.make_async_copy(gain, gain_v, own_sem.at[7]),
         pltpu.make_async_copy(w_key, kv_in.at[0], own_sem.at[0]),
         pltpu.make_async_copy(w_value, kv_in.at[1], own_sem.at[1]),
         pltpu.make_async_copy(w_out, wfull.at[s, t], own_sem.at[2]),
@@ -216,34 +218,43 @@
         pltpu.make_async_copy(w_pool, wp, own_sem.at[4]),
         pltpu.make_async_copy(cos_all.at[pl.ds(pl.multiple_of(s * blocks, blocks), blocks)], cos_at, own_sem.at[5]),
         pltpu.make_async_copy(sin_all.at[pl.ds(pl.multiple_of(s * blocks, blocks), blocks)], sin_at, own_sem.at[6]),
+        pltpu.make_async_copy(cos_in, cos_v, own_sem.at[8]),
+        pltpu.make_async_copy(sin_in, sin_v, own_sem.at[9]),
+        pltpu.make_async_copy(scale, scale_v, own_sem.at[10]),
+        pltpu.make_async_copy(sink, sink_v, own_sem.at[11]),
     ]
     barrier = pltpu.get_barrier_semaphore()
     greet = [(((z + d) % Z) * 4 + s % 4, t) for d in range(1, Z)]
-    greet += [(yflip, t), (after, t), (before, t), (s, cross)]
+    greet += [(yflip, t), (after, t), (before, t), (s, cross), (yflip, cross)]
     for to_s, to_t in greet:
         pl.semaphore_signal(barrier, inc=1, device_id={"sp": to_s, "tp": to_t}, device_id_type=MESH)
-    for copy in own_copies[:3]:
+    for copy in own_copies[:6]:
         copy.start()
-    tok_copies[0].start()
-    for copy in own_copies[3:]:
+    tok_copy(0).start()
+    for copy in own_copies[6:]:
         copy.start()
-    for copy in tok_copies[1:]:
-        copy.start()
+    for i in range(1, chunks):
+        tok_copy(i).start()
 
     lane = lax.broadcasted_iota(jnp.int32, (QB, LANES), 1)
     low_half = lane < HEAD
     first_half = lane % HEAD < HEAD // 2
 
     own_copies[0].wait()
+    gains = jnp.transpose(jnp.concatenate([gain_v[...]] * (LANES // gain.shape[0]), axis=0))
+
+    def gain_column(b):
+        return pltpu.roll(gains, (LANES - b) % LANES, 1)[:, :1]
+
     own_copies[1].wait()
+    own_copies[2].wait()
     key_head = t * local_heads // (QH // KVH)
     key_in = kv_in[0].astype(jnp.float32)
     value_in = kv_in[1].astype(jnp.float32)
     key_cols = jnp.where(key_head == 0, key_in, pltpu.roll(key_in, HEAD, 1))
     value_cols = jnp.where(key_head == 0, pltpu.roll(value_in, HEAD, 1), value_in)
-    kvw[s] = jnp.where(low_half, key_cols, value_cols).astype(jnp.bfloat16)
-    own_copies[2].wait()
-    pl.semaphore_wait(barrier, len(greet))
+    kvw[s] = (jnp.where(low_half, key_cols, value_cols) * gain_column(s)).astype(jnp.bfloat16)
+    own_copies[3].wait()
 
     pending = []
 
@@ -274,7 +285,7 @@
     def wo_copy(b, half, send, to_s, to_t):
         return lambda: remote(wfull.at[b, half], wfull.at[b, half], send, wo_recv.at[b, half], to_s, to_t)
 
-    hop = [1, -1, 2, -2]
+    hop = [2, -2, 1, -1]
 
     def at_z(d):
         return s + 4 * d
@@ -314,13 +325,11 @@
 
     ev = {}
     ev["kv_own"] = event(None, None,
-        [(here(h), kv_copy(s, kz_send.at[i], at_z(h))) for i, h in enumerate(hop) if abs(h) < Z]
+        [(here(h), kv_copy(s, kz_send.at[i], at_z(h))) for i, h in enumerate(far)]
         + [(None, kv_copy(s, ko_send.at[0], yflip)), (None, kv_copy(s, ko_send.at[1], partner))])
     for i, d in enumerate(far):
         step, fine = onward(d)
         items = [(None, kv_copy(at_z(d), kf_send.at[i, 0], yflip)), (None, kv_copy(at_z(d), kf_send.at[i, 1], partner))]
-        if 2 <= abs(d) < Z - 1:
-            items = [(fine, kv_copy(at_z(d), kf_send.at[i, 2], at_z(step)))] + items
         ev["kv", d] = event(here(d), kv_copy(at_z(d), kf_send.at[i, 0], yflip), items)
     for i, d in enumerate([0] + far):
         ev["kvy", d] = event(None if d == 0 else here(d), kv_copy(at_yz(d), ky_send.at[i], partner),
@@ -329,17 +338,18 @@
     ev["wo_own"] = event(None, None,
         [(None, wo_copy(s, t, wo_send.at[0], s, cross)), (None, wo_copy(s, t, wo_send.at[1], yflip, t))]
         + [(here(h), wo_copy(s, t, wz_send.at[i], at_z(h), t)) for i, h in enumerate(hop) if abs(h) < Z]
-        + [(None, wo_copy(s, t, wo_send.at[2], partner, t))])
-    ev["wo_x"] = event(None, wo_copy(s, cross, wx_send.at[0], yflip, t),
-        [(None, wo_copy(s, cross, wx_send.at[0], yflip, t)), (None, wo_copy(s, cross, wx_send.at[1], partner, t))])
+        + [(None, wo_copy(s, t, wo_send.at[3], yflip, cross)), (None, wo_copy(s, t, wo_send.at[2], partner, t))])
+    ev["wo_x"] = event(None, wo_copy(s, cross, wx_send.at[1], partner, t),
+        [(None, wo_copy(s, cross, wx_send.at[1], partner, t))])
     ev["wo_d"] = event(None, wo_copy(yflip, cross, wd_send.at[4], partner, t),
         [(here(h), wo_copy(yflip, cross, wd_send.at[i], at_z(h), t)) for i, h in enumerate(hop) if abs(h) < Z]
         + [(None, wo_copy(yflip, cross, wd_send.at[4], partner, t))])
     for i, d in enumerate(far):
         step, fine = onward(d)
         b = at_z(d)
-        items = [(None, wo_copy(b, t, w00_send.at[i, 0], s, cross)), (None, wo_copy(b, t, w00_send.at[i, 1], yflip, t)),
-                 (None, wo_copy(b, t, w00_send.at[i, 2], partner, t))]
+        items = [(None, wo_copy(b, t, w00_send.at[i, 1], yflip, t)), (None, wo_copy(b, t, w00_send.at[i, 2], partner, t))]
+        if abs(d) != 2:
+            items = [(None, wo_copy(b, t, w00_send.at[i, 0], s, cross))] + items
         if 2 <= abs(d) < Z - 1:
             items = [(fine, wo_copy(b, t, w00_send.at[i, 3], at_z(step), t))] + items
         ev["w00", d] = event(here(d), wo_copy(b, t, w00_send.at[i, 0], s, cross), items)
@@ -349,6 +359,8 @@
         items = [(None, wo_copy(b, cross, w11_send.at[i, 0], partner, t))]
         if 2 <= abs(d) < Z - 1:
             items = [(fine, wo_copy(b, cross, w11_send.at[i, 1], at_z(step), t))] + items
+        if abs(d) == 2:
+            items = items + [(None, wo_copy(b, cross, w11_send.at[i, 2], yflip, t))]
         ev["w11", d] = event(here(d), wo_copy(b, cross, w11_send.at[i, 0], partner, t), items)
     for i, d in enumerate([0] + far):
         b = at_yz(d)
@@ -361,14 +373,22 @@
                 if abs(d) < Z:
                     ev[kind, d]()
 
-    ev["kv_own"]()
-    ev["wo_own"]()
+    def begin():
+        pl.semaphore_wait(barrier, len(greet))
+        ev["kv_own"]()
+        ev["wo_own"]()
+
+    late = z > 0
+
+    @pl.when(late)
+    def _():
+        begin()
 
     def rotated(values, b):
         ca = cos_at[pl.ds(b, 1), :]
         sa = sin_at[pl.ds(b, 1), :]
-        ci = cos_in[...]
-        si = sin_in[...]
+        ci = cos_v[...]
+        si = sin_v[...]
         cosine = ca * ci - sa * si
         sine = sa * ci + ca * si
         swapped = jnp.where(
@@ -378,132 +398,26 @@
         )
         return values * cosine + swapped * sine
 
-    for copy in own_copies[3:]:
+    for copy in own_copies[4:6]:
         copy.wait()
-    LN = 32
-
-    def project(i, carry):
-        base = pl.multiple_of(i * CHUNK, CHUNK)
-        pltpu.make_async_copy(
-            tokens.at[pl.ds(base, CHUNK)], tok.at[pl.ds(base, CHUNK)], tok_sem.at[i]
-        ).wait()
-
-        def norm(r, carry):
-            at = pl.multiple_of(base + r * LN, LN)
-            values = tok[pl.ds(at, LN), :].astype(jnp.float32)
-            center = jnp.sum(values, axis=1, keepdims=True) * (1.0 / width)
-            moved = values - center
-            spread = jnp.sum(moved * moved, axis=1, keepdims=True) * (1.0 / width)
-            normed[pl.ds(at, LN), :] = (moved * lax.rsqrt(spread + 1e-06) * gain[...]).astype(
-                jnp.bfloat16
-            )
-            return carry
-
-        lax.fori_loop(0, CHUNK // LN, norm, 0, unroll=2)
-        part = normed[pl.ds(base, CHUNK), :]
-        query = jnp.dot(part, wq[...], preferred_element_type=jnp.float32)
-        for k in range(CHUNK // QB):
-            b = i * (CHUNK // QB) + k
-            for g in range(groups):
-                turned = rotated(query[k * QB:(k + 1) * QB, g * LANES:(g + 1) * LANES], b) * HEAD ** (-0.5)
-                qs[b, pl.ds(2 * g * QB, QB), :] = jnp.where(low_half, turned, 0.0).astype(jnp.bfloat16)
-                qs[b, pl.ds((2 * g + 1) * QB, QB), :] = jnp.where(
-                    low_half, pltpu.roll(turned, HEAD, 1), 0.0
-                ).astype(jnp.bfloat16)
-        mixed = jnp.dot(part, wp[...], preferred_element_type=jnp.float32)
-        pool[pl.ds(pl.multiple_of(reach + base, 8), CHUNK), :] = mixed.astype(jnp.bfloat16).astype(jnp.float32)
-
-
-        @pl.when(i == 1)
-        def _():
-            poll("kv", 1)
-
-        @pl.when(i == 2)
-        def _():
-            poll("kv", 2)
-            poll("kvy", 0)
-            ev["wo_x"]()
-
-        @pl.when(i == 3)
-        def _():
-            poll("kv", *range(3, Z))
-            poll("kvy", 1)
-            poll("w00", 1)
-        return carry
-
-    lax.fori_loop(0, chunks, project, 0)
-
-    inner = s < S - 1
-    outer = s > 0
-    halo_pool = [
-        (inner, lambda: remote(pool.at[pl.ds(rows, reach)], pool.at[pl.ds(0, reach)], halo_send.at[0], halo_recv.at[0], after, t)),
-        (outer, lambda: remote(pool.at[pl.ds(reach, reach)], pool.at[pl.ds(rows + reach, reach)], halo_send.at[1], halo_recv.at[1], before, t)),
-    ]
-    halo_kv = [
-        (inner, lambda: remote(kv.at[pl.ds(rows, WINDOW)], kv.at[pl.ds(0, WINDOW)], halo_send.at[2], halo_recv.at[2], after, t)),
-        (outer, lambda: remote(kv.at[pl.ds(WINDOW, WINDOW)], kv.at[pl.ds(rows + WINDOW, WINDOW)], halo_send.at[3], halo_recv.at[3], before, t)),
-    ]
-    pending.extend(halo_pool + halo_kv)
-
-    def halo_wait(pair):
-        @pl.when(outer)
-        def _():
-            pair[0][1]().wait_recv()
-
-        @pl.when(inner)
-        def _():
-            pair[1][1]().wait_recv()
-
-    start_all(halo_pool)
-
-    @pl.when(s == 0)
-    def _():
-        pool[0:reach, :] = jnp.zeros((reach, pool.shape[1]), jnp.float32)
-        kv[0:WINDOW, :] = jnp.zeros((WINDOW, LANES), jnp.bfloat16)
-
-    @pl.when(s == S - 1)
-    def _():
-        pool[rows + reach:rows + 2 * reach, :] = jnp.zeros((reach, pool.shape[1]), jnp.float32)
-        kv[rows + WINDOW:rows + 2 * WINDOW, :] = jnp.zeros((WINDOW, LANES), jnp.bfloat16)
-
-    poll("kvy", *range(2, Z))
-    own_core = [s] + [at_z(d) for d in far] + [yflip] + [at_yz(d) for d in far]
-    arrives = [(None, partner), (None, yflip + partner - s)]
-    arrives += [(here(d), partner + 4 * d) for d in far] + [(here(d), yflip + partner - s + 4 * d) for d in far]
-    for cond, b in arrives:
-        make = kv_copy(b, ko_send.at[1], partner)
-        if cond is None:
-            make().wait_recv()
-        else:
-            @pl.when(cond)
-            def _(make=make):
-                make().wait_recv()
-
-    def key_value(j, carry):
-        i = jnp.where(j == 0, 0, jnp.where(j == 1, chunks - 1, j - 1))
-        base = pl.multiple_of(i * CHUNK, CHUNK)
-        both = jnp.dot(
-            normed[pl.ds(base, CHUNK), :], kvw[...].reshape(width, LANES), preferred_element_type=jnp.float32
-        )
-        for k in range(CHUNK // QB):
-            piece = both[k * QB:(k + 1) * QB, :]
-            turned = rotated(piece, i * (CHUNK // QB) + k)
-            kv[pl.ds(pl.multiple_of(WINDOW + base + k * QB, QB), QB), :] = jnp.where(
-                low_half, turned, piece
-            ).astype(jnp.bfloat16)
-
-        @pl.when(j == 0)
-        def _():
-            ev["wo_d"]()
-
-        @pl.when(j == 2)
-        def _():
-            start_all(halo_kv)
-            poll("w00", 2)
-        return carry
-
-    lax.fori_loop(0, chunks, key_value, 0)
-    halo_wait(halo_pool)
+    wide = w_query.shape[1]
+
+    def fold(b, carry):
+        at = pl.ds(pl.multiple_of(b * LANES, LANES), LANES)
+        column = gain_column(b)
+        sums = []
+        for k, part in enumerate((wq, wp)):
+            scaled = (part[at, :].astype(jnp.float32) * column).astype(jnp.bfloat16)
+            wqp[at, k * wide:(k + 1) * wide] = scaled
+            sums.append(jnp.sum(scaled.astype(jnp.float32).reshape(LANES // 8, 8, wide), axis=0))
+        return carry + jnp.concatenate(sums, axis=1)
+
+    folded = lax.fori_loop(0, width // LANES, fold, jnp.zeros((8, 2 * wide), jnp.float32), unroll=2)
+    total_qp = jnp.sum(folded, axis=0, keepdims=True)
+    for copy in own_copies[6:]:
+        copy.wait()
+    LN = 16
+    hc = chunks // 2
 
     def pooled(b, g):
         cols = slice(g * LANES, (g + 1) * LANES)
@@ -523,32 +437,165 @@
             wide = jnp.where(index == k, span // 2, wide)
         pos = offset + b * QB + lax.broadcasted_iota(jnp.int32, (QB, LANES), 0)
         counted = (jnp.minimum(pos + wide, total_rows) - jnp.maximum(pos - wide, 0)).astype(jnp.float32)
-        return ((picked / counted - values[reach:reach + QB]) * scale[:, cols]).astype(jnp.bfloat16)
-
-    def pool_other(i, carry):
+        return ((picked / counted - values[reach:reach + QB]) * scale_v[:, cols]).astype(jnp.bfloat16)
+
+
+    def ex_pool(n):
+        at = pl.ds(pl.multiple_of(n * QB, QB), QB)
+        return remote(pool_send.at[at], joined.at[T + t, at], exp_send.at[n], exp_recv.at[n], s, cross)
+
+    def ex_att(n):
+        at = pl.ds(pl.multiple_of(n * QB, QB), QB)
+        return remote(att_send.at[at], joined.at[t, at], exa_send.at[n], exa_recv.at[n], s, cross)
+
+    def send_pooled(n):
         for g in range(pgroups):
-            pool_send[pl.ds(pl.multiple_of(i * QB, QB), QB), g * LANES:(g + 1) * LANES] = pooled(cross * hb + i, g)
+            pool_send[pl.ds(pl.multiple_of(n * QB, QB), QB), g * LANES:(g + 1) * LANES] = pooled(cross * hb + n, g)
+        ex_pool(n).start()
+
+    def project(i, carry):
+        base = chunk_at(i)
+        tok_copy(i).wait()
+        raw = jnp.dot(tok[pl.ds(base, CHUNK), :], wqp[...], preferred_element_type=jnp.float32)
+        scales = []
+        shifts = []
+        for r in range(CHUNK // LN):
+            at = pl.ds(pl.multiple_of(base + r * LN, LN), LN)
+            values = tok[at, :].astype(jnp.float32)
+            center = jnp.sum(values, axis=1, keepdims=True) * (1.0 / width)
+            moved = values - center
+            spread = jnp.sum(moved * moved, axis=1, keepdims=True) * (1.0 / width)
+            inverse = lax.rsqrt(spread + 1e-06)
+            scales.append(inverse)
+            shifts.append(center * inverse)
+        rstd = jnp.broadcast_to(jnp.concatenate(scales, axis=0), (CHUNK, LANES))
+        drop = jnp.broadcast_to(jnp.concatenate(shifts, axis=0), (CHUNK, LANES))
+        scale_at[pl.ds(base, CHUNK), :] = rstd
+        shift_at[pl.ds(base, CHUNK), :] = drop
+
+        def normal(k, g):
+            at = slice(k * QB, (k + 1) * QB)
+            cols = slice(g * LANES, (g + 1) * LANES)
+            return raw[at, cols] * rstd[at] - drop[at] * total_qp[:, cols]
+
+        for k in range(CHUNK // QB):
+            b = base // QB + k
+            for g in range(groups):
+                turned = rotated(normal(k, g), b) * HEAD ** (-0.5)
+                qs[b, pl.ds(2 * g * QB, QB), :] = jnp.where(low_half, turned, 0.0).astype(jnp.bfloat16)
+                qs[b, pl.ds((2 * g + 1) * QB, QB), :] = jnp.where(
+                    low_half, pltpu.roll(turned, HEAD, 1), 0.0
+                ).astype(jnp.bfloat16)
+            for g in range(pgroups):
+                pool[pl.ds(pl.multiple_of(reach + base + k * QB, 8), QB), g * LANES:(g + 1) * LANES] = (
+                    normal(k, groups + g).astype(jnp.bfloat16).astype(jnp.float32)
+                )
+
+        @pl.when((i == 0) & (z == 0))
+        def _():
+            begin()
+
+        @pl.when(i == hc - 1)
+        def _():
+            for n in range(1, hb - 1):
+                send_pooled(n)
+
+        @pl.when(i == hc)
+        def _():
+            send_pooled(jnp.where(t == 0, 0, hb - 1))
+            poll("kv", *range(1, Z))
+
+        @pl.when(i == chunks - 1)
+        def _():
+            ev["wo_x"]()
+            poll("w01", 0)
         return carry
+
+    lax.fori_loop(0, chunks, project, 0)
+
+    inner = s < S - 1
+    outer = s > 0
+    halo_pool = [
+        (inner, lambda: remote(pool.at[pl.ds(rows, reach)], pool.at[pl.ds(0, reach)], halo_send.at[0], halo_recv.at[0], after, t)),
+        (outer, lambda: remote(pool.at[pl.ds(reach, reach)], pool.at[pl.ds(rows + reach, reach)], halo_send.at[1], halo_recv.at[1], before, t)),
+    ]
+    halo_kv = [
+        (inner, lambda: remote(kv.at[pl.ds(rows, WINDOW)], kv.at[pl.ds(0, WINDOW)], halo_send.at[2], halo_recv.at[2], after, t)),
+        (outer, lambda: remote(kv.at[pl.ds(WINDOW, WINDOW)], kv.at[pl.ds(rows + WINDOW, WINDOW)], halo_send.at[3], halo_recv.at[3], before, t)),
+    ]
+    pending.extend(halo_pool + halo_kv)
+
+    def halo_wait(pair):
+        @pl.when(outer)
+        def _():
+            pair[0][1]().wait_recv()
+
+        @pl.when(inner)
+        def _():
+            pair[1][1]().wait_recv()
+
+    start_all(halo_pool)
+
+    @pl.when(s == 0)
+    def _():
+        pool[0:reach, :] = jnp.zeros((reach, pool.shape[1]), jnp.float32)
+        kv[0:WINDOW, :] = jnp.zeros((WINDOW, LANES), jnp.bfloat16)
+
+    @pl.when(s == S - 1)
+    def _():
+        pool[rows + reach:rows + 2 * reach, :] = jnp.zeros((reach, pool.shape[1]), jnp.float32)
+        kv[rows + WINDOW:rows + 2 * WINDOW, :] = jnp.zeros((WINDOW, LANES), jnp.bfloat16)
 
     def pool_own(i, carry):
         for g in range(pgroups):
             joined[T + t, pl.ds(pl.multiple_of(i * QB, QB), QB), g * LANES:(g + 1) * LANES] = pooled(t * hb + i, g)
         return carry
 
-
-    ex_pool = (None, lambda: remote(pool_send, joined.at[T + t], exp_send.at[0], exp_recv.at[0], s, cross))
-    pending.append(ex_pool)
-
-    def ex_att(n):
-        at = pl.ds(pl.multiple_of(n * QB, QB), QB)
-        return remote(att_send.at[at], joined.at[t, at], exa_send.at[n], exa_recv.at[n], s, cross)
-
-    lax.fori_loop(0, hb, pool_other, 0)
-    ex_pool[1]().start()
-    poll("w00", *range(3, Z))
+    halo_wait(halo_pool)
+    send_pooled(jnp.where(t == 0, hb - 1, 0))
+    poll("kvy", *range(Z))
+    poll("w00", 2)
     lax.fori_loop(0, hb, pool_own, 0)
-    poll("w10", 1)
-    poll("w01", 0, 1)
+    arrives = [(None, partner), (None, yflip + partner - s)]
+    arrives += [(here(d), partner + 4 * d) for d in far] + [(here(d), yflip + partner - s + 4 * d) for d in far]
+    for cond, b in arrives:
+        make = kv_copy(b, ko_send.at[1], partner)
+        if cond is None:
+            make().wait_recv()
+        else:
+            @pl.when(cond)
+            def _(make=make):
+                make().wait_recv()
+
+    def gather_sum(b, carry):
+        return carry + jnp.sum(kvw[b].astype(jnp.float32).reshape(LANES // 8, 8, LANES), axis=0)
+
+    total_kv = jnp.sum(
+        lax.fori_loop(0, S, gather_sum, jnp.zeros((8, LANES), jnp.float32), unroll=4), axis=0, keepdims=True
+    )
+
+    def key_value(j, carry):
+        i = jnp.where(j == 0, 0, jnp.where(j == 1, chunks - 1, j - 1))
+        base = pl.multiple_of(i * CHUNK, CHUNK)
+        both = jnp.dot(
+            tok[pl.ds(base, CHUNK), :], kvw[...].reshape(width, LANES), preferred_element_type=jnp.float32
+        )
+        both = both * scale_at[pl.ds(base, CHUNK), :] - shift_at[pl.ds(base, CHUNK), :] * total_kv
+        for k in range(CHUNK // QB):
+            piece = both[k * QB:(k + 1) * QB, :]
+            turned = rotated(piece, i * (CHUNK // QB) + k)
+            kv[pl.ds(pl.multiple_of(WINDOW + base + k * QB, QB), QB), :] = jnp.where(
+                low_half, turned, piece
+            ).astype(jnp.bfloat16)
+
+        @pl.when(j == 1)
+        def _():
+            start_all(halo_kv)
+            ev["wo_d"]()
+            poll("w00", 1)
+        return carry
+
+    lax.fori_loop(0, chunks, key_value, 0)
 
     span = QB + 2 * WINDOW
     row_id = lax.broadcasted_iota(jnp.int32, (QB, span), 0)
@@ -567,9 +614,9 @@
         norms = []
         for h in range(local_heads):
             part = jnp.where(valid, scores[h * QB:(h + 1) * QB], NEG_BIG)
-            top = jnp.maximum(jnp.max(part, axis=1, keepdims=True), sink[h])
+            top = jnp.maximum(jnp.max(part, axis=1, keepdims=True), sink_v[h])
             expo = jnp.exp(part - top)
-            norms.append(1.0 / (jnp.sum(expo, axis=1, keepdims=True) + jnp.exp(sink[h] - top)))
+            norms.append(1.0 / (jnp.sum(expo, axis=1, keepdims=True) + jnp.exp(sink_v[h] - top)))
             expos.append(expo.astype(jnp.bfloat16))
         result = jnp.dot(jnp.concatenate(expos, axis=0), context, preferred_element_type=jnp.float32)
         heads = [result[h * QB:(h + 1) * QB] * norms[h] for h in range(local_heads)]
@@ -590,9 +637,10 @@
             att_send[pl.ds(at, QB), g * LANES:(g + 1) * LANES] = value
         ex_att(n).start()
 
-        @pl.when(i == 1)
-        def _():
-            poll("w11", 1)
+        @pl.when(i == hb - 1)
+        def _():
+            poll("w01", 2)
+            poll("w00", *range(3, Z))
         return carry
 
     def attend_own(i, carry):
@@ -601,35 +649,39 @@
         for g, value in enumerate(attend(b)):
             joined[t, pl.ds(at, QB), g * LANES:(g + 1) * LANES] = value
 
-        @pl.when(i == 0)
-        def _():
-            poll("w10", 2)
-            poll("w01", 2)
-
-        @pl.when(i == 2)
+        @pl.when(i == 1)
+        def _():
+            poll("w01", 1)
+            poll("w10", 1)
+
+        @pl.when(i == hb - 1)
         def _():
             poll("w11", 2)
         return carry
 
     lax.fori_loop(0, hb, attend_other, 0)
     lax.fori_loop(0, hb, attend_own, 0)
-    poll("w10", *range(3, Z))
-    poll("w01", *range(3, Z))
-
-    remote(pool_send, joined.at[T + cross], exp_send.at[0], exp_recv.at[0], s, cross).wait_recv()
-    wide = joined.shape[2]
+    for n in range(hb):
+        at = pl.ds(n * QB, QB)
+        remote(pool_send.at[at], joined.at[T + cross, at], exp_send.at[n], exp_recv.at[n], s, cross).wait_recv()
 
     def columns(n, half, start, count):
         at = pl.ds(pl.multiple_of(start, wide), count)
         return jnp.concatenate([wfull[2 * n, half, at, :], wfull[2 * n + 1, half, at, :]], axis=1)
 
     def most(j, carry):
-        over = j // Z
+        @pl.when(j == 0)
+        def _():
+            poll("w11", 1)
+
         @pl.when(j == 2)
         def _():
+            poll("w01", *range(3, Z))
+            poll("w10", *range(2, Z))
             poll("w11", *range(3, Z))
+        over = j % 2
         side = y + over - 2 * y * over
-        k = j % Z
+        k = j // 2
         zz = jnp.where(z < Z // 2, (z + k) % Z, (z + Z - k) % Z)
         n = zz * 2 + side
         for half in range(T):
@@ -661,6 +713,7 @@
             def _(make=make):
                 make().wait_send()
     for n in range(hb):
+        ex_pool(n).wait_send()
         ex_att(n).wait_send()
 
 
@@ -675,6 +728,7 @@
         and w_query.shape[1] % LANES == 0 and w_pool_in.shape[1] % LANES == 0
         and w_query.shape[1] == w_pool_in.shape[1]
         and local_heads == QH // KVH and rows % (2 * CHUNK) == 0
+        and width == S * LANES and LANES % S == 0
     )
     if not fits:
         return plain_body(
@@ -688,20 +742,26 @@
     reach = POOL_SPANS[-1] // 2
     wide = w_query.shape[1]
     vmem = pl.BlockSpec(memory_space=pltpu.VMEM)
-    smem = pl.BlockSpec(memory_space=pltpu.SMEM)
     hbm = pl.BlockSpec(memory_space=pltpu.HBM)
     dma = pltpu.SemaphoreType.DMA
     bf = jnp.bfloat16
     return pl.pallas_call(
         functools.partial(mixer_kernel, (S, T)),
         out_shape=pltpu.VMEM((half, S * w_out.shape[1]), bf),
-        in_specs=[hbm, vmem, hbm, hbm, hbm, hbm, smem, vmem, hbm, vmem, vmem, hbm, hbm],
+        in_specs=[hbm] * 13,
         out_specs=vmem,
         scratch_shapes=[
-            pltpu.VMEM((rows, width), bf),
+            pltpu.VMEM((width // LANES, LANES), jnp.float32),
+            pltpu.VMEM((1, wide), jnp.float32),
+            pltpu.SMEM(sink_logit.shape, jnp.float32),
+            pltpu.VMEM((QB, LANES), jnp.float32),
+            pltpu.VMEM((QB, LANES), jnp.float32),
             pltpu.VMEM((rows, width), bf),
             pltpu.VMEM(w_query.shape, bf),
             pltpu.VMEM(w_pool_in.shape, bf),
+            pltpu.VMEM((width, 2 * wide), bf),
+            pltpu.VMEM((rows, LANES), jnp.float32),
+            pltpu.VMEM((rows, LANES), jnp.float32),
             pltpu.VMEM((2,) + w_key.shape, bf),
             pltpu.VMEM((S, LANES, LANES), bf),
             pltpu.VMEM((S, T) + w_out.shape, bf),
@@ -715,25 +775,25 @@
             pltpu.VMEM((blocks, LANES), jnp.float32),
             pltpu.VMEM((blocks, LANES), jnp.float32),
             dma((rows // CHUNK,)),
-            dma((7,)),
+            dma((12,)),
             dma((S,)),
-            dma((4,)),
+            dma((F,)),
             dma((2,)),
-            dma((F, 3)),
+            dma((F, 2)),
             dma((F + 1,)),
             dma((S, T)),
             dma((4,)),
-            dma((3,)),
+            dma((4,)),
             dma((2,)),
             dma((5,)),
             dma((F, 4)),
             dma((F,)),
             dma((F + 1,)),
-            dma((F, 2)),
+            dma((F, 3)),
             dma((4,)),
             dma((4,)),
-            dma((1,)),
-            dma((1,)),
+            dma((blocks // 2,)),
+            dma((blocks // 2,)),
             dma((blocks // 2,)),
             dma((blocks // 2,)),
         ],
@@ -741,7 +801,7 @@
             collective_id=0, has_side_effects=True, vmem_limit_bytes=VMEM_LIMIT
         ),
     )(
-        tokens, norm_gain[None, :], w_query, w_key, w_value, w_pool_in, sink_logit, pool_scale[None, :], w_out, *tables
+        tokens, norm_gain.reshape(width // LANES, LANES), w_query, w_key, w_value, w_pool_in, sink_logit, pool_scale[None, :], w_out, *tables
     )
 
 

time: 45.4 us -> 41 us (0.903)
  Pallas kernels: 43.9 us -> 39.5 us
    pallas_call x1, Pallas kernels: 43.9 us -> 39.5 us  [body(): pl.pallas_call(functools.partial(mixer_kernel, (S, T)), out_shape=pltpu.V...]
where the time goes in v2:
time: 41 us; the launch traced here: 40.8 us
  Pallas kernels  39.5 us (96%)
  local copies, waits for them, and re-layouts  1.32 us (3%)
    pallas_call x1, Pallas kernels, body(): pl.pallas_call(functools.partial(mixer_kernel, (S, T)), out_shape=pltpu.V...  39.5 us
    unnamed x1, local copies, waits for them, and re-layouts  1.32 us

profile of v2, /device:TPU:0, one launch (start us, length us, event | category | flops | bytes accessed | tf_op | source)
XLA Modules:
  0.0 40.8 jit_solution(11590708777393559350)
XLA Ops:
  0.0 39.5 %shard_map.127 = bf16[512,2048]{1,0:T(8,128)(2,1)S(1)} custom-call(bf16[1024,2048]{1,0:T(8,128)(2,1)} %tokens.1, f32[16,128]{1,0:T(8,128)} %bitcast.2, bf16[2048,256]{1,0:T(8,128)(2,1)} %w_query.1, bf16[128,128]{1,0:T(8,128)(2,1)} %w_key.1, bf16[128,128]{1,0:T(8,128)(2,1)} %w_value.1, bf16[2048,256]{1,0:T(8,128)(2,1)} %w_pool.1, f32[4]{0:T(128)} %sink.1, ...), custom_call_target="tpu_custom_call" | custom-call | tf_op jit(solution)/shard_map/pallas_call | solution.py:748
  39.5 1.3 %copy.15 = bf16[512,2048]{1,0:T(8,128)(2,1)} copy(bf16[512,2048]{1,0:T(8,128)(2,1)S(1)} %shard_map.127) | data formatting | bytes 4194304

commit v3 on v2

--- a/solution.py
+++ b/solution.py
@@ -166,7 +166,7 @@
 def mixer_kernel(
     places, tokens, gain, w_query, w_key, w_value, w_pool, sink, scale, w_out, cos_in, sin_in, cos_all, sin_all,
     out,
-    gain_v, scale_v, sink_v, cos_v, sin_v, tok, wq, wp, wqp, scale_at, shift_at, kv_in, kvw, wfull, qs, kv, pool, pool_send, att_send, joined, acc, cos_at, sin_at,
+    tok_halo, gain_v, scale_v, sink_v, cos_v, sin_v, tok, wq, wp, wqp, scale_at, shift_at, kv_in, kvw, wfull, qs, kv, pool, pool_send, att_send, joined, acc, cos_at, sin_at,
     tok_sem, own_sem, kv_recv, kz_send, ko_send, kf_send, ky_send,
     wo_recv, wz_send, wo_send, wx_send, wd_send, w00_send, w10_send, w01_send, w11_send,
     halo_send, halo_recv, exp_send, exp_recv, exa_send, exa_recv,
@@ -336,20 +336,21 @@
             [(None, kv_copy(at_yz(d), ky_send.at[i], partner))])
 
     ev["wo_own"] = event(None, None,
-        [(None, wo_copy(s, t, wo_send.at[0], s, cross)), (None, wo_copy(s, t, wo_send.at[1], yflip, t))]
-        + [(here(h), wo_copy(s, t, wz_send.at[i], at_z(h), t)) for i, h in enumerate(hop) if abs(h) < Z]
-        + [(None, wo_copy(s, t, wo_send.at[3], yflip, cross)), (None, wo_copy(s, t, wo_send.at[2], partner, t))])
-    ev["wo_x"] = event(None, wo_copy(s, cross, wx_send.at[1], partner, t),
-        [(None, wo_copy(s, cross, wx_send.at[1], partner, t))])
+        [(None, wo_copy(s, t, wo_send.at[0], s, cross)), (None, wo_copy(s, t, wo_send.at[1], yflip, t)),
+         (None, wo_copy(s, t, wo_send.at[2], partner, t))])
+    ev["wo_own_z"] = event(None, None,
+        [(here(h), wo_copy(s, t, wz_send.at[i], at_z(h), t)) for i, h in enumerate(hop) if abs(h) < Z])
+    ev["wo_x"] = event(None, wo_copy(s, cross, wx_send.at[0], yflip, t),
+        [(None, wo_copy(s, cross, wx_send.at[0], yflip, t)), (None, wo_copy(s, cross, wx_send.at[1], partner, t))])
     ev["wo_d"] = event(None, wo_copy(yflip, cross, wd_send.at[4], partner, t),
         [(here(h), wo_copy(yflip, cross, wd_send.at[i], at_z(h), t)) for i, h in enumerate(hop) if abs(h) < Z]
         + [(None, wo_copy(yflip, cross, wd_send.at[4], partner, t))])
     for i, d in enumerate(far):
         step, fine = onward(d)
         b = at_z(d)
-        items = [(None, wo_copy(b, t, w00_send.at[i, 1], yflip, t)), (None, wo_copy(b, t, w00_send.at[i, 2], partner, t))]
-        if abs(d) != 2:
-            items = [(None, wo_copy(b, t, w00_send.at[i, 0], s, cross))] + items
+        items = [(None, wo_copy(b, t, w00_send.at[i, 2], partner, t))]
+        ev["w00y", d] = event(here(d), None, [(None, wo_copy(b, t, w00_send.at[i, 1], yflip, t))])
+        items = [(None, wo_copy(b, t, w00_send.at[i, 0], s, cross))] + items
         if 2 <= abs(d) < Z - 1:
             items = [(fine, wo_copy(b, t, w00_send.at[i, 3], at_z(step), t))] + items
         ev["w00", d] = event(here(d), wo_copy(b, t, w00_send.at[i, 0], s, cross), items)
@@ -359,8 +360,6 @@
         items = [(None, wo_copy(b, cross, w11_send.at[i, 0], partner, t))]
         if 2 <= abs(d) < Z - 1:
             items = [(fine, wo_copy(b, cross, w11_send.at[i, 1], at_z(step), t))] + items
-        if abs(d) == 2:
-            items = items + [(None, wo_copy(b, cross, w11_send.at[i, 2], yflip, t))]
         ev["w11", d] = event(here(d), wo_copy(b, cross, w11_send.at[i, 0], partner, t), items)
     for i, d in enumerate([0] + far):
         b = at_yz(d)
@@ -373,8 +372,40 @@
                 if abs(d) < Z:
                     ev[kind, d]()
 
+    inner = s < S - 1
+    outer = s > 0
+    halo_tok = [
+        (inner, lambda: remote(tokens.at[pl.ds(rows - reach, reach)], tok_halo.at[0], halo_send.at[0], halo_recv.at[0], after, t)),
+        (outer, lambda: remote(tokens.at[pl.ds(0, reach)], tok_halo.at[1], halo_send.at[1], halo_recv.at[1], before, t)),
+    ]
+    halo_kv = [
+        (inner, lambda: remote(kv.at[pl.ds(rows, WINDOW)], kv.at[pl.ds(0, WINDOW)], halo_send.at[2], halo_recv.at[2], after, t)),
+        (outer, lambda: remote(kv.at[pl.ds(WINDOW, WINDOW)], kv.at[pl.ds(rows + WINDOW, WINDOW)], halo_send.at[3], halo_recv.at[3], before, t)),
+    ]
+    pending.extend(halo_tok + halo_kv)
+
+    def halo_wait(pair):
+        @pl.when(outer)
+        def _():
+            pair[0][1]().wait_recv()
+
+        @pl.when(inner)
+        def _():
+            pair[1][1]().wait_recv()
+
+    @pl.when(s == 0)
+    def _():
+        tok_halo[0] = jnp.zeros((reach, width), jnp.bfloat16)
+        kv[0:WINDOW, :] = jnp.zeros((WINDOW, LANES), jnp.bfloat16)
+
+    @pl.when(s == S - 1)
+    def _():
+        tok_halo[1] = jnp.zeros((reach, width), jnp.bfloat16)
+        kv[rows + WINDOW:rows + 2 * WINDOW, :] = jnp.zeros((WINDOW, LANES), jnp.bfloat16)
+
     def begin():
         pl.semaphore_wait(barrier, len(greet))
+        start_all(halo_tok)
         ev["kv_own"]()
         ev["wo_own"]()
 
@@ -414,6 +445,7 @@
 
     folded = lax.fori_loop(0, width // LANES, fold, jnp.zeros((8, 2 * wide), jnp.float32), unroll=2)
     total_qp = jnp.sum(folded, axis=0, keepdims=True)
+
     for copy in own_copies[6:]:
         copy.wait()
     LN = 16
@@ -453,6 +485,14 @@
             pool_send[pl.ds(pl.multiple_of(n * QB, QB), QB), g * LANES:(g + 1) * LANES] = pooled(cross * hb + n, g)
         ex_pool(n).start()
 
+    def moments(rows_in):
+        values = rows_in.astype(jnp.float32)
+        center = jnp.sum(values, axis=1, keepdims=True) * (1.0 / width)
+        moved = values - center
+        spread = jnp.sum(moved * moved, axis=1, keepdims=True) * (1.0 / width)
+        inverse = lax.rsqrt(spread + 1e-06)
+        return inverse, center * inverse
+
     def project(i, carry):
         base = chunk_at(i)
         tok_copy(i).wait()
@@ -461,13 +501,9 @@
         shifts = []
         for r in range(CHUNK // LN):
             at = pl.ds(pl.multiple_of(base + r * LN, LN), LN)
-            values = tok[at, :].astype(jnp.float32)
-            center = jnp.sum(values, axis=1, keepdims=True) * (1.0 / width)
-            moved = values - center
-            spread = jnp.sum(moved * moved, axis=1, keepdims=True) * (1.0 / width)
-            inverse = lax.rsqrt(spread + 1e-06)
+            inverse, shifted = moments(tok[at, :])
             scales.append(inverse)
-            shifts.append(center * inverse)
+            shifts.append(shifted)
         rstd = jnp.broadcast_to(jnp.concatenate(scales, axis=0), (CHUNK, LANES))
         drop = jnp.broadcast_to(jnp.concatenate(shifts, axis=0), (CHUNK, LANES))
         scale_at[pl.ds(base, CHUNK), :] = rstd
@@ -495,6 +531,10 @@
         def _():
             begin()
 
+        @pl.when(i == jnp.where(z == 0, 1, 0))
+        def _():
+            ev["wo_own_z"]()
+
         @pl.when(i == hc - 1)
         def _():
             for n in range(1, hb - 1):
@@ -504,58 +544,31 @@
         def _():
             send_pooled(jnp.where(t == 0, 0, hb - 1))
             poll("kv", *range(1, Z))
-
-        @pl.when(i == chunks - 1)
-        def _():
             ev["wo_x"]()
-            poll("w01", 0)
+
         return carry
 
     lax.fori_loop(0, chunks, project, 0)
 
-    inner = s < S - 1
-    outer = s > 0
-    halo_pool = [
-        (inner, lambda: remote(pool.at[pl.ds(rows, reach)], pool.at[pl.ds(0, reach)], halo_send.at[0], halo_recv.at[0], after, t)),
-        (outer, lambda: remote(pool.at[pl.ds(reach, reach)], pool.at[pl.ds(rows + reach, reach)], halo_send.at[1], halo_recv.at[1], before, t)),
-    ]
-    halo_kv = [
-        (inner, lambda: remote(kv.at[pl.ds(rows, WINDOW)], kv.at[pl.ds(0, WINDOW)], halo_send.at[2], halo_recv.at[2], after, t)),
-        (outer, lambda: remote(kv.at[pl.ds(WINDOW, WINDOW)], kv.at[pl.ds(rows + WINDOW, WINDOW)], halo_send.at[3], halo_recv.at[3], before, t)),
-    ]
-    pending.extend(halo_pool + halo_kv)
-
-    def halo_wait(pair):
-        @pl.when(outer)
-        def _():
-            pair[0][1]().wait_recv()
-
-        @pl.when(inner)
-        def _():
-            pair[1][1]().wait_recv()
-
-    start_all(halo_pool)
-
-    @pl.when(s == 0)
-    def _():
-        pool[0:reach, :] = jnp.zeros((reach, pool.shape[1]), jnp.float32)
-        kv[0:WINDOW, :] = jnp.zeros((WINDOW, LANES), jnp.bfloat16)
-
-    @pl.when(s == S - 1)
-    def _():
-        pool[rows + reach:rows + 2 * reach, :] = jnp.zeros((reach, pool.shape[1]), jnp.float32)
-        kv[rows + WINDOW:rows + 2 * WINDOW, :] = jnp.zeros((WINDOW, LANES), jnp.bfloat16)
+    halo_wait(halo_tok)
+    edge = jnp.concatenate([tok_halo[0], tok_halo[1]], axis=0)
+    edge_scale, edge_shift = moments(edge)
+    edge_pool = (
+        jnp.dot(edge, wqp[:, wide:], preferred_element_type=jnp.float32) * edge_scale - edge_shift * total_qp[:, wide:]
+    ).astype(jnp.bfloat16).astype(jnp.float32)
+    pool[0:reach, :] = edge_pool[:reach]
+    pool[rows + reach:rows + 2 * reach, :] = edge_pool[reach:]
 
     def pool_own(i, carry):
+        n = jnp.where(t == 0, i, hb - 1 - i)
         for g in range(pgroups):
-            joined[T + t, pl.ds(pl.multiple_of(i * QB, QB), QB), g * LANES:(g + 1) * LANES] = pooled(t * hb + i, g)
+            joined[T + t, pl.ds(pl.multiple_of(n * QB, QB), QB), g * LANES:(g + 1) * LANES] = pooled(t * hb + n, g)
         return carry
 
-    halo_wait(halo_pool)
     send_pooled(jnp.where(t == 0, hb - 1, 0))
+    lax.fori_loop(0, hb, pool_own, 0)
     poll("kvy", *range(Z))
     poll("w00", 2)
-    lax.fori_loop(0, hb, pool_own, 0)
     arrives = [(None, partner), (None, yflip + partner - s)]
     arrives += [(here(d), partner + 4 * d) for d in far] + [(here(d), yflip + partner - s + 4 * d) for d in far]
     for cond, b in arrives:
@@ -574,9 +587,8 @@
         lax.fori_loop(0, S, gather_sum, jnp.zeros((8, LANES), jnp.float32), unroll=4), axis=0, keepdims=True
     )
 
-    def key_value(j, carry):
-        i = jnp.where(j == 0, 0, jnp.where(j == 1, chunks - 1, j - 1))
-        base = pl.multiple_of(i * CHUNK, CHUNK)
+    def key_value(i):
+        base = i * CHUNK
         both = jnp.dot(
             tok[pl.ds(base, CHUNK), :], kvw[...].reshape(width, LANES), preferred_element_type=jnp.float32
         )
@@ -584,18 +596,18 @@
         for k in range(CHUNK // QB):
             piece = both[k * QB:(k + 1) * QB, :]
             turned = rotated(piece, i * (CHUNK // QB) + k)
-            kv[pl.ds(pl.multiple_of(WINDOW + base + k * QB, QB), QB), :] = jnp.where(
-                low_half, turned, piece
-            ).astype(jnp.bfloat16)
-
-        @pl.when(j == 1)
-        def _():
-            start_all(halo_kv)
-            ev["wo_d"]()
-            poll("w00", 1)
-        return carry
-
-    lax.fori_loop(0, chunks, key_value, 0)
+            kv[pl.ds(WINDOW + base + k * QB, QB), :] = jnp.where(low_half, turned, piece).astype(jnp.bfloat16)
+
+    key_value(0)
+    key_value(chunks - 1)
+    start_all(halo_kv)
+    poll("w00y", 2)
+    poll("w00", 1)
+    for i in range(1, chunks - 1):
+        key_value(i)
+    ev["wo_d"]()
+    poll("w01", 0)
+    poll("w00y", 1)
 
     span = QB + 2 * WINDOW
     row_id = lax.broadcasted_iota(jnp.int32, (QB, span), 0)
@@ -637,10 +649,6 @@
             att_send[pl.ds(at, QB), g * LANES:(g + 1) * LANES] = value
         ex_att(n).start()
 
-        @pl.when(i == hb - 1)
-        def _():
-            poll("w01", 2)
-            poll("w00", *range(3, Z))
         return carry
 
     def attend_own(i, carry):
@@ -649,14 +657,21 @@
         for g, value in enumerate(attend(b)):
             joined[t, pl.ds(at, QB), g * LANES:(g + 1) * LANES] = value
 
-        @pl.when(i == 1)
-        def _():
+        @pl.when(i == 0)
+        def _():
+            poll("w00", *range(3, Z))
+            poll("w00y", *range(3, Z))
+
+        @pl.when(i == 2)
+        def _():
+            poll("w11", 2)
+
+        @pl.when(i == hb - 1)
+        def _():
+            poll("w01", 2)
+            poll("w10", 2)
             poll("w01", 1)
             poll("w10", 1)
-
-        @pl.when(i == hb - 1)
-        def _():
-            poll("w11", 2)
         return carry
 
     lax.fori_loop(0, hb, attend_other, 0)
@@ -669,42 +684,62 @@
         at = pl.ds(pl.multiple_of(start, wide), count)
         return jnp.concatenate([wfull[2 * n, half, at, :], wfull[2 * n + 1, half, at, :]], axis=1)
 
-    def most(j, carry):
-        @pl.when(j == 0)
-        def _():
-            poll("w11", 1)
-
-        @pl.when(j == 2)
-        def _():
-            poll("w01", *range(3, Z))
-            poll("w10", *range(2, Z))
-            poll("w11", *range(3, Z))
+    def chunk_of(j):
         over = j % 2
         side = y + over - 2 * y * over
         k = j // 2
         zz = jnp.where(z < Z // 2, (z + k) % Z, (z + Z - k) % Z)
-        n = zz * 2 + side
+        return zz * 2 + side
+
+    def chunk_wait(n):
         for half in range(T):
             piece = wfull.at[2 * n + 1 - c, half]
             remote(piece, piece, wo_send.at[2], wo_recv.at[2 * n + 1 - c, half], partner, t).wait_recv()
+
+    def store(n, total):
+        out[:, pl.ds(pl.multiple_of(n * 2 * LANES, 2 * LANES), 2 * LANES)] = total.astype(jnp.bfloat16)
+
+    def most(j, carry):
+        @pl.when(j == 1)
+        def _():
+            poll("w11", 1)
+        n = chunk_of(j)
+        chunk_wait(n)
         left = jnp.concatenate([joined[t]] + [joined[T + k] for k in range(T)], axis=1)
         right = jnp.concatenate([columns(n, 0, t * wide, wide), columns(n, 1, 0, T * wide)], axis=0)
         acc[n] = jnp.dot(left, right, preferred_element_type=jnp.float32)
         return carry
 
-    lax.fori_loop(0, S // 2, most, 0)
+    def last(j, carry):
+        n = chunk_of(j)
+        store(n, acc[n] + jnp.dot(
+            joined[cross], columns(n, 0, cross * wide, wide), preferred_element_type=jnp.float32
+        ))
+        return carry
+
+    def whole(j, carry):
+        @pl.when(j == split)
+        def _():
+            poll("w01", *range(3, Z))
+            poll("w11", *range(3, Z))
+
+        @pl.when(j == split + 1)
+        def _():
+            poll("w10", *range(3, Z))
+        n = chunk_of(j)
+        chunk_wait(n)
+        left = jnp.concatenate([joined[k] for k in range(2 * T)], axis=1)
+        right = jnp.concatenate([columns(n, half, 0, T * wide) for half in range(T)], axis=0)
+        store(n, jnp.dot(left, right, preferred_element_type=jnp.float32))
+        return carry
+
+    split = S // 4
+    lax.fori_loop(0, split, most, 0)
     for n in range(hb):
         at = pl.ds(n * QB, QB)
         remote(att_send.at[at], joined.at[cross, at], exa_send.at[n], exa_recv.at[n], s, cross).wait_recv()
-
-    def last(n, carry):
-        total = acc[n] + jnp.dot(
-            joined[cross], columns(n, 0, cross * wide, wide), preferred_element_type=jnp.float32
-        )
-        out[:, pl.ds(pl.multiple_of(n * 2 * LANES, 2 * LANES), 2 * LANES)] = total.astype(jnp.bfloat16)
-        return carry
-
-    lax.fori_loop(0, S // 2, last, 0)
+    lax.fori_loop(0, split, last, 0)
+    lax.fori_loop(split, S // 2, whole, 0)
     for cond, make in pending:
         if cond is None:
             make().wait_send()
@@ -751,6 +786,7 @@
         in_specs=[hbm] * 13,
         out_specs=vmem,
         scratch_shapes=[
+            pltpu.VMEM((2, reach, width), bf),
             pltpu.VMEM((width // LANES, LANES), jnp.float32),
             pltpu.VMEM((1, wide), jnp.float32),
             pltpu.SMEM(sink_logit.shape, jnp.float32),

time: 41 us -> 37.1 us (0.905)
  Pallas kernels: 39.5 us -> 35.4 us
    pallas_call x1, Pallas kernels: 39.5 us -> 35.4 us  [body(): pl.pallas_call(functools.partial(mixer_kernel, (S, T)), out_shape=pltpu.V...]
where the time goes in v3:
time: 37.1 us; the launch traced here: 36.7 us
  Pallas kernels  35.4 us (95%)
  local copies, waits for them, and re-layouts  1.32 us (4%)
    pallas_call x1, Pallas kernels, body(): pl.pallas_call(functools.partial(mixer_kernel, (S, T)), out_shape=pltpu.V...  35.4 us
    unnamed x1, local copies, waits for them, and re-layouts  1.32 us

profile of v3, /device:TPU:0, one launch (start us, length us, event | category | flops | bytes accessed | tf_op | source)
XLA Modules:
  0.0 36.7 jit_solution(17144511588850533149)
XLA Ops:
  0.0 35.4 %shard_map.127 = bf16[512,2048]{1,0:T(8,128)(2,1)S(1)} custom-call(bf16[1024,2048]{1,0:T(8,128)(2,1)} %tokens.1, f32[16,128]{1,0:T(8,128)} %bitcast.2, bf16[2048,256]{1,0:T(8,128)(2,1)} %w_query.1, bf16[128,128]{1,0:T(8,128)(2,1)} %w_key.1, bf16[128,128]{1,0:T(8,128)(2,1)} %w_value.1, bf16[2048,256]{1,0:T(8,128)(2,1)} %w_pool.1, f32[4]{0:T(128)} %sink.1, ...), custom_call_target="tpu_custom_call" | custom-call | tf_op jit(solution)/shard_map/pallas_call | solution.py:783
  35.4 1.3 %copy.15 = bf16[512,2048]{1,0:T(8,128)(2,1)} copy(bf16[512,2048]{1,0:T(8,128)(2,1)S(1)} %shard_map.127) | data formatting | bytes 4194304

commit v4 on v3

--- a/solution.py
+++ b/solution.py
@@ -167,9 +167,7 @@
     places, tokens, gain, w_query, w_key, w_value, w_pool, sink, scale, w_out, cos_in, sin_in, cos_all, sin_all,
     out,
     tok_halo, gain_v, scale_v, sink_v, cos_v, sin_v, tok, wq, wp, wqp, scale_at, shift_at, kv_in, kvw, wfull, qs, kv, pool, pool_send, att_send, joined, acc, cos_at, sin_at,
-    tok_sem, own_sem, kv_recv, kz_send, ko_send, kf_send, ky_send,
-    wo_recv, wz_send, wo_send, wx_send, wd_send, w00_send, w10_send, w01_send, w11_send,
-    halo_send, halo_recv, exp_send, exp_recv, exa_send, exa_recv,
+    tok_sem, own_sem, kv_send, kv_recv, wo_send, wo_recv, wp_recv, halo_send, halo_recv, ex_send, ex_recv,
 ):
     S, T = places
     Z = S // 4
@@ -256,34 +254,22 @@
     kvw[s] = (jnp.where(low_half, key_cols, value_cols) * gain_column(s)).astype(jnp.bfloat16)
     own_copies[3].wait()
 
-    pending = []
-
-    def go(cond, make):
-        pending.append((cond, make))
-        if cond is None:
-            make().start()
-        else:
-            @pl.when(cond)
-            def _():
-                make().start()
-
-    def later(cond, make):
-        pending.append((cond, make))
-
     def here(d):
         return (z + d >= 0) & (z + d < Z)
 
-    def piece_kv(b):
-        return kvw.at[b]
-
-    def piece_wo(b, half):
-        return wfull.at[b, half]
-
-    def kv_copy(b, send, to):
-        return lambda: remote(kvw.at[b], kvw.at[b], send, kv_recv.at[b], to, t)
-
-    def wo_copy(b, half, send, to_s, to_t):
-        return lambda: remote(wfull.at[b, half], wfull.at[b, half], send, wo_recv.at[b, half], to_s, to_t)
+    def kv_copy(b, link, to):
+        return lambda: remote(kvw.at[b], kvw.at[b], kv_send.at[0], kv_recv.at[link], to, t)
+
+    def kv_wait(link, count):
+        some = kvw.at[pl.ds(0, count)]
+        remote(some, some, kv_send.at[0], kv_recv.at[link], partner, t).wait_recv()
+
+    def wo_copy(b, half, group, to_s, to_t):
+        return lambda: remote(wfull.at[b, half], wfull.at[b, half], wo_send.at[group], wo_recv.at[b // 2, half], to_s, to_t)
+
+    def hand(b, half, group=0):
+        return (None, lambda: remote(
+            wfull.at[b, half], wfull.at[b, half], wo_send.at[group], wp_recv.at[b // 4], partner, t))
 
     hop = [2, -2, 1, -1]
 
@@ -292,9 +278,6 @@
 
     def at_yz(d):
         return yflip + 4 * d
-
-    def reach_index(d):
-        return far.index(d)
 
     def start_all(items):
         for cond, make in items:
@@ -306,8 +289,6 @@
                     make().start()
 
     def event(cond, arrival, items):
-        pending.extend([(cond if k is None else (k if cond is None else cond & k), m) for k, m in items])
-
         def act():
             def inner():
                 if arrival is not None:
@@ -325,46 +306,41 @@
 
     ev = {}
     ev["kv_own"] = event(None, None,
-        [(here(h), kv_copy(s, kz_send.at[i], at_z(h))) for i, h in enumerate(far)]
-        + [(None, kv_copy(s, ko_send.at[0], yflip)), (None, kv_copy(s, ko_send.at[1], partner))])
-    for i, d in enumerate(far):
+        [(here(h), kv_copy(s, 0, at_z(h))) for h in far]
+        + [(None, kv_copy(s, 1, yflip)), (None, kv_copy(s, 2, partner))])
+    kv_to_y = [(here(d), kv_copy(at_z(d), 1, yflip)) for d in far]
+    kv_to_p = [(here(d), kv_copy(at_z(d), 2, partner)) for d in far]
+    kv_y_to_p = [(None, kv_copy(yflip, 2, partner))] + [(here(d), kv_copy(at_yz(d), 2, partner)) for d in far]
+
+    ev["wo_own"] = event(None, None,
+        [(None, wo_copy(s, t, 0, s, cross)), (z > 0, wo_copy(s, t, 0, yflip, t)), hand(s, t, 2)])
+    ev["wo_own_y"] = event(None, None, [(z == 0, wo_copy(s, t, 0, yflip, t))])
+    ahead = [(h, here(h) & here(2 * h) if abs(h) == 1 else here(h)) for h in hop if abs(h) < Z]
+    ends = [(h, here(h) & jnp.logical_not(here(2 * h))) for h in hop if abs(h) == 1]
+    ev["wo_own_z"] = event(None, None, [(ok, wo_copy(s, t, 1, at_z(h), t)) for h, ok in ahead])
+    ev["wo_own_end"] = event(None, None, [(ok, wo_copy(s, t, 1, at_z(h), t)) for h, ok in ends])
+    ev["wo_x"] = event(None, wo_copy(s, cross, 0, yflip, t),
+        [(None, wo_copy(s, cross, 0, yflip, t)), hand(s, cross)])
+    ev["wo_d"] = event(None, wo_copy(yflip, cross, 0, partner, t),
+        [(ok, wo_copy(yflip, cross, 1, at_z(h), t)) for h, ok in ahead] + [hand(yflip, cross)])
+    ev["wo_d_end"] = event(None, None, [(ok, wo_copy(yflip, cross, 1, at_z(h), t)) for h, ok in ends])
+    for d in far:
         step, fine = onward(d)
-        items = [(None, kv_copy(at_z(d), kf_send.at[i, 0], yflip)), (None, kv_copy(at_z(d), kf_send.at[i, 1], partner))]
-        ev["kv", d] = event(here(d), kv_copy(at_z(d), kf_send.at[i, 0], yflip), items)
-    for i, d in enumerate([0] + far):
-        ev["kvy", d] = event(None if d == 0 else here(d), kv_copy(at_yz(d), ky_send.at[i], partner),
-            [(None, kv_copy(at_yz(d), ky_send.at[i], partner))])
-
-    ev["wo_own"] = event(None, None,
-        [(None, wo_copy(s, t, wo_send.at[0], s, cross)), (None, wo_copy(s, t, wo_send.at[1], yflip, t)),
-         (None, wo_copy(s, t, wo_send.at[2], partner, t))])
-    ev["wo_own_z"] = event(None, None,
-        [(here(h), wo_copy(s, t, wz_send.at[i], at_z(h), t)) for i, h in enumerate(hop) if abs(h) < Z])
-    ev["wo_x"] = event(None, wo_copy(s, cross, wx_send.at[0], yflip, t),
-        [(None, wo_copy(s, cross, wx_send.at[0], yflip, t)), (None, wo_copy(s, cross, wx_send.at[1], partner, t))])
-    ev["wo_d"] = event(None, wo_copy(yflip, cross, wd_send.at[4], partner, t),
-        [(here(h), wo_copy(yflip, cross, wd_send.at[i], at_z(h), t)) for i, h in enumerate(hop) if abs(h) < Z]
-        + [(None, wo_copy(yflip, cross, wd_send.at[4], partner, t))])
-    for i, d in enumerate(far):
-        step, fine = onward(d)
+        relay = 2 <= abs(d) < Z - 1
         b = at_z(d)
-        items = [(None, wo_copy(b, t, w00_send.at[i, 2], partner, t))]
-        ev["w00y", d] = event(here(d), None, [(None, wo_copy(b, t, w00_send.at[i, 1], yflip, t))])
-        items = [(None, wo_copy(b, t, w00_send.at[i, 0], s, cross))] + items
-        if 2 <= abs(d) < Z - 1:
-            items = [(fine, wo_copy(b, t, w00_send.at[i, 3], at_z(step), t))] + items
-        ev["w00", d] = event(here(d), wo_copy(b, t, w00_send.at[i, 0], s, cross), items)
-        ev["w10", d] = event(here(d), wo_copy(b, cross, w10_send.at[i], partner, t),
-            [(None, wo_copy(b, cross, w10_send.at[i], partner, t))])
+        items = [(None, wo_copy(b, t, 0, s, cross)), (None, wo_copy(b, t, 0, yflip, t)), hand(b, t)]
+        if relay:
+            items = [(fine, wo_copy(b, t, 1, at_z(step), t))] + items
+        ev["w00", d] = event(here(d), wo_copy(b, t, 0, s, cross), items)
+        ev["w10", d] = event(here(d), wo_copy(b, cross, 0, partner, t), [hand(b, cross)])
         b = at_yz(d)
-        items = [(None, wo_copy(b, cross, w11_send.at[i, 0], partner, t))]
-        if 2 <= abs(d) < Z - 1:
-            items = [(fine, wo_copy(b, cross, w11_send.at[i, 1], at_z(step), t))] + items
-        ev["w11", d] = event(here(d), wo_copy(b, cross, w11_send.at[i, 0], partner, t), items)
-    for i, d in enumerate([0] + far):
+        items = [hand(b, cross)]
+        if relay:
+            items = [(fine, wo_copy(b, cross, 1, at_z(step), t))] + items
+        ev["w11", d] = event(here(d), wo_copy(b, cross, 0, partner, t), items)
+    for d in [0] + far:
         b = at_yz(d)
-        ev["w01", d] = event(None if d == 0 else here(d), wo_copy(b, t, w01_send.at[i], partner, t),
-            [(None, wo_copy(b, t, w01_send.at[i], partner, t))])
+        ev["w01", d] = event(None if d == 0 else here(d), wo_copy(b, t, 0, partner, t), [hand(b, t)])
 
     def poll(kind, *distances):
         for k in distances:
@@ -382,7 +358,6 @@
         (inner, lambda: remote(kv.at[pl.ds(rows, WINDOW)], kv.at[pl.ds(0, WINDOW)], halo_send.at[2], halo_recv.at[2], after, t)),
         (outer, lambda: remote(kv.at[pl.ds(WINDOW, WINDOW)], kv.at[pl.ds(rows + WINDOW, WINDOW)], halo_send.at[3], halo_recv.at[3], before, t)),
     ]
-    pending.extend(halo_tok + halo_kv)
 
     def halo_wait(pair):
         @pl.when(outer)
@@ -405,8 +380,8 @@
 
     def begin():
         pl.semaphore_wait(barrier, len(greet))
+        ev["kv_own"]()
         start_all(halo_tok)
-        ev["kv_own"]()
         ev["wo_own"]()
 
     late = z > 0
@@ -474,11 +449,11 @@
 
     def ex_pool(n):
         at = pl.ds(pl.multiple_of(n * QB, QB), QB)
-        return remote(pool_send.at[at], joined.at[T + t, at], exp_send.at[n], exp_recv.at[n], s, cross)
+        return remote(pool_send.at[at], joined.at[T + t, at], ex_send.at[0], ex_recv.at[0], s, cross)
 
     def ex_att(n):
         at = pl.ds(pl.multiple_of(n * QB, QB), QB)
-        return remote(att_send.at[at], joined.at[t, at], exa_send.at[n], exa_recv.at[n], s, cross)
+        return remote(att_send.at[at], joined.at[t, at], ex_send.at[1], ex_recv.at[1], s, cross)
 
     def send_pooled(n):
         for g in range(pgroups):
@@ -543,8 +518,15 @@
         @pl.when(i == hc)
         def _():
             send_pooled(jnp.where(t == 0, 0, hb - 1))
-            poll("kv", *range(1, Z))
+            kv_wait(0, Z - 1)
+            start_all(kv_to_y)
+            start_all(kv_to_p)
+            ev["wo_own_end"]()
+
+        @pl.when(i == jnp.where(z == 0, chunks - 1, hc))
+        def _():
             ev["wo_x"]()
+            ev["wo_own_y"]()
 
         return carry
 
@@ -567,18 +549,9 @@
 
     send_pooled(jnp.where(t == 0, hb - 1, 0))
     lax.fori_loop(0, hb, pool_own, 0)
-    poll("kvy", *range(Z))
-    poll("w00", 2)
-    arrives = [(None, partner), (None, yflip + partner - s)]
-    arrives += [(here(d), partner + 4 * d) for d in far] + [(here(d), yflip + partner - s + 4 * d) for d in far]
-    for cond, b in arrives:
-        make = kv_copy(b, ko_send.at[1], partner)
-        if cond is None:
-            make().wait_recv()
-        else:
-            @pl.when(cond)
-            def _(make=make):
-                make().wait_recv()
+    kv_wait(1, Z)
+    start_all(kv_y_to_p)
+    kv_wait(2, 2 * Z)
 
     def gather_sum(b, carry):
         return carry + jnp.sum(kvw[b].astype(jnp.float32).reshape(LANES // 8, 8, LANES), axis=0)
@@ -601,13 +574,12 @@
     key_value(0)
     key_value(chunks - 1)
     start_all(halo_kv)
-    poll("w00y", 2)
+    poll("w00", 2)
+    ev["wo_d"]()
     poll("w00", 1)
     for i in range(1, chunks - 1):
         key_value(i)
-    ev["wo_d"]()
-    poll("w01", 0)
-    poll("w00y", 1)
+    ev["wo_d_end"]()
 
     span = QB + 2 * WINDOW
     row_id = lax.broadcasted_iota(jnp.int32, (QB, span), 0)
@@ -660,96 +632,104 @@
         @pl.when(i == 0)
         def _():
             poll("w00", *range(3, Z))
-            poll("w00y", *range(3, Z))
 
         @pl.when(i == 2)
         def _():
+            poll("w01", 0)
             poll("w11", 2)
 
-        @pl.when(i == hb - 1)
-        def _():
-            poll("w01", 2)
-            poll("w10", 2)
-            poll("w01", 1)
-            poll("w10", 1)
         return carry
 
     lax.fori_loop(0, hb, attend_other, 0)
     lax.fori_loop(0, hb, attend_own, 0)
-    for n in range(hb):
-        at = pl.ds(n * QB, QB)
-        remote(pool_send.at[at], joined.at[T + cross, at], exp_send.at[n], exp_recv.at[n], s, cross).wait_recv()
+    whole_pool = remote(pool_send, joined.at[T + cross], ex_send.at[0], ex_recv.at[0], s, cross)
+    whole_att = remote(att_send, joined.at[cross], ex_send.at[1], ex_recv.at[1], s, cross)
+    whole_pool.wait_recv()
 
     def columns(n, half, start, count):
         at = pl.ds(pl.multiple_of(start, wide), count)
         return jnp.concatenate([wfull[2 * n, half, at, :], wfull[2 * n + 1, half, at, :]], axis=1)
 
-    def chunk_of(j):
-        over = j % 2
-        side = y + over - 2 * y * over
-        k = j // 2
-        zz = jnp.where(z < Z // 2, (z + k) % Z, (z + Z - k) % Z)
-        return zz * 2 + side
-
-    def chunk_wait(n):
-        for half in range(T):
-            piece = wfull.at[2 * n + 1 - c, half]
-            remote(piece, piece, wo_send.at[2], wo_recv.at[2 * n + 1 - c, half], partner, t).wait_recv()
+    def pair_of(p):
+        zz = jnp.where(z < Z // 2, (z + p) % Z, (z + Z - p) % Z)
+        return [zz * 2 + y, zz * 2 + 1 - y]
+
+    def pair_wait(pair):
+        some = wfull.at[pl.ds(0, 2)]
+        remote(some, some, wo_send.at[2], wp_recv.at[pair[0] // 2], partner, t).wait_recv()
+
+    def pair_columns(pair, half, start, count):
+        return jnp.concatenate([columns(n, half, start, count) for n in pair], axis=1)
 
     def store(n, total):
         out[:, pl.ds(pl.multiple_of(n * 2 * LANES, 2 * LANES), 2 * LANES)] = total.astype(jnp.bfloat16)
 
-    def most(j, carry):
-        @pl.when(j == 1)
-        def _():
+    def most(p, carry):
+        @pl.when(p == 1)
+        def _():
+            poll("w10", 1)
             poll("w11", 1)
-        n = chunk_of(j)
-        chunk_wait(n)
+            poll("w01", 1)
+        pair = pair_of(p)
+        pair_wait(pair)
         left = jnp.concatenate([joined[t]] + [joined[T + k] for k in range(T)], axis=1)
-        right = jnp.concatenate([columns(n, 0, t * wide, wide), columns(n, 1, 0, T * wide)], axis=0)
-        acc[n] = jnp.dot(left, right, preferred_element_type=jnp.float32)
+        right = jnp.concatenate([pair_columns(pair, 0, t * wide, wide), pair_columns(pair, 1, 0, T * wide)], axis=0)
+        total = jnp.dot(left, right, preferred_element_type=jnp.float32)
+        acc[pair[0]] = total[:, :2 * LANES]
+        acc[pair[1]] = total[:, 2 * LANES:]
         return carry
 
-    def last(j, carry):
-        n = chunk_of(j)
-        store(n, acc[n] + jnp.dot(
-            joined[cross], columns(n, 0, cross * wide, wide), preferred_element_type=jnp.float32
-        ))
+    def last(p, carry):
+        pair = pair_of(p)
+        total = jnp.dot(
+            joined[cross], pair_columns(pair, 0, cross * wide, wide), preferred_element_type=jnp.float32
+        )
+        store(pair[0], acc[pair[0]] + total[:, :2 * LANES])
+        store(pair[1], acc[pair[1]] + total[:, 2 * LANES:])
         return carry
 
-    def whole(j, carry):
-        @pl.when(j == split)
-        def _():
-            poll("w01", *range(3, Z))
+    def whole(p, carry):
+        @pl.when(p == split)
+        def _():
+            poll("w10", *range(3, Z))
             poll("w11", *range(3, Z))
-
-        @pl.when(j == split + 1)
-        def _():
-            poll("w10", *range(3, Z))
-        n = chunk_of(j)
-        chunk_wait(n)
+        pair = pair_of(p)
+        pair_wait(pair)
         left = jnp.concatenate([joined[k] for k in range(2 * T)], axis=1)
-        right = jnp.concatenate([columns(n, half, 0, T * wide) for half in range(T)], axis=0)
-        store(n, jnp.dot(left, right, preferred_element_type=jnp.float32))
+        right = jnp.concatenate([pair_columns(pair, half, 0, T * wide) for half in range(T)], axis=0)
+        total = jnp.dot(left, right, preferred_element_type=jnp.float32)
+        store(pair[0], total[:, :2 * LANES])
+        store(pair[1], total[:, 2 * LANES:])
         return carry
 
-    split = S // 4
+    split = Z // 2
     lax.fori_loop(0, split, most, 0)
-    for n in range(hb):
-        at = pl.ds(n * QB, QB)
-        remote(att_send.at[at], joined.at[cross, at], exa_send.at[n], exa_recv.at[n], s, cross).wait_recv()
+    poll("w01", *range(2, Z))
+    poll("w10", 2)
+    whole_att.wait_recv()
     lax.fori_loop(0, split, last, 0)
-    lax.fori_loop(split, S // 2, whole, 0)
-    for cond, make in pending:
-        if cond is None:
+    lax.fori_loop(split, Z, whole, 0)
+
+    def sent(ref, sem):
+        remote(ref, ref, sem, halo_recv.at[0], partner, t).wait_send()
+
+    for cond, make in halo_tok + halo_kv:
+        @pl.when(cond)
+        def _(make=make):
             make().wait_send()
-        else:
-            @pl.when(cond)
-            def _(make=make):
-                make().wait_send()
-    for n in range(hb):
-        ex_pool(n).wait_send()
-        ex_att(n).wait_send()
+    whole_pool.wait_send()
+    whole_att.wait_send()
+    sent(kvw.at[pl.ds(0, 4 * Z - 1)], kv_send.at[0])
+    sent(wfull.at[s, t], wo_send.at[2])
+    sent(wfull.at[pl.ds(0, 3 * Z)], wo_send.at[0])
+    for at in range(Z):
+        inside = lambda k: 0 <= k < Z
+        count = sum(inside(at + h) for h in hop)
+        count += sum(inside(at + d) and inside(at - d // abs(d)) for d in far if 2 <= abs(d) < Z - 1)
+
+        @pl.when(z == at)
+        def _(count=count):
+            sent(wfull.at[pl.ds(0, count)], wo_send.at[1])
 
 
 def body(mesh, tokens, norm_gain, w_query, w_key, w_value, w_pool_in, sink_logit, pool_scale, w_out):
@@ -773,7 +753,6 @@
     blocks = rows // QB
     half = rows // T
     Z = S // 4
-    F = 2 * (Z - 1)
     reach = POOL_SPANS[-1] // 2
     wide = w_query.shape[1]
     vmem = pl.BlockSpec(memory_space=pltpu.VMEM)
@@ -812,26 +791,15 @@
             pltpu.VMEM((blocks, LANES), jnp.float32),
             dma((rows // CHUNK,)),
             dma((12,)),
-            dma((S,)),
-            dma((F,)),
-            dma((2,)),
-            dma((F, 2)),
-            dma((F + 1,)),
-            dma((S, T)),
+            dma((1,)),
+            dma((3,)),
+            dma((3,)),
+            dma((S // 2, T)),
+            dma((Z,)),
             dma((4,)),
             dma((4,)),
             dma((2,)),
-            dma((5,)),
-            dma((F, 4)),
-            dma((F,)),
-            dma((F + 1,)),
-            dma((F, 3)),
-            dma((4,)),
-            dma((4,)),
-            dma((blocks // 2,)),
-            dma((blocks // 2,)),
-            dma((blocks // 2,)),
-            dma((blocks // 2,)),
+            dma((2,)),
         ],
         compiler_params=pltpu.CompilerParams(
             collective_id=0, has_side_effects=True, vmem_limit_bytes=VMEM_LIMIT

time: 37.1 us -> 36.5 us (0.984)
  Pallas kernels: 35.4 us -> 35 us
where the time goes in v4:
time: 36.5 us; the launch traced here: 36.3 us
  Pallas kernels  35 us (96%)
  local copies, waits for them, and re-layouts  1.32 us (4%)
    pallas_call x1, Pallas kernels, body(): pl.pallas_call(functools.partial(mixer_kernel, (S, T)), out_shape=pltpu.V...  35 us
    unnamed x1, local copies, waits for them, and re-layouts  1.32 us

profile of v4, /device:TPU:0, one launch (start us, length us, event | category | flops | bytes accessed | tf_op | source)
XLA Modules:
  0.0 36.3 jit_solution(441542234005535462)
XLA Ops:
  0.0 35.0 %shard_map.127 = bf16[512,2048]{1,0:T(8,128)(2,1)S(1)} custom-call(bf16[1024,2048]{1,0:T(8,128)(2,1)} %tokens.1, f32[16,128]{1,0:T(8,128)} %bitcast.2, bf16[2048,256]{1,0:T(8,128)(2,1)} %w_query.1, bf16[128,128]{1,0:T(8,128)(2,1)} %w_key.1, bf16[128,128]{1,0:T(8,128)(2,1)} %w_value.1, bf16[2048,256]{1,0:T(8,128)(2,1)} %w_pool.1, f32[4]{0:T(128)} %sink.1, ...), custom_call_target="tpu_custom_call" | custom-call | tf_op jit(solution)/shard_map/pallas_call | solution.py:762
  35.0 1.3 %copy.15 = bf16[512,2048]{1,0:T(8,128)(2,1)} copy(bf16[512,2048]{1,0:T(8,128)(2,1)S(1)} %shard_map.127) | data formatting | bytes 4194304

commit v5 on v4

--- a/solution.py
+++ b/solution.py
@@ -313,34 +313,46 @@
     kv_y_to_p = [(None, kv_copy(yflip, 2, partner))] + [(here(d), kv_copy(at_yz(d), 2, partner)) for d in far]
 
     ev["wo_own"] = event(None, None,
-        [(None, wo_copy(s, t, 0, s, cross)), (z > 0, wo_copy(s, t, 0, yflip, t)), hand(s, t, 2)])
+        [(None, wo_copy(s, t, 2, s, cross)), (z > 0, wo_copy(s, t, 0, yflip, t)), hand(s, t, 2)])
     ev["wo_own_y"] = event(None, None, [(z == 0, wo_copy(s, t, 0, yflip, t))])
     ahead = [(h, here(h) & here(2 * h) if abs(h) == 1 else here(h)) for h in hop if abs(h) < Z]
     ends = [(h, here(h) & jnp.logical_not(here(2 * h))) for h in hop if abs(h) == 1]
     ev["wo_own_z"] = event(None, None, [(ok, wo_copy(s, t, 1, at_z(h), t)) for h, ok in ahead])
     ev["wo_own_end"] = event(None, None, [(ok, wo_copy(s, t, 1, at_z(h), t)) for h, ok in ends])
+    def rim(d):
+        return here(d) & ((z == 0) | (z == Z - 1) | (z + d == 0) | (z + d == Z - 1))
+
     ev["wo_x"] = event(None, wo_copy(s, cross, 0, yflip, t),
-        [(None, wo_copy(s, cross, 0, yflip, t)), hand(s, cross)])
+        [(None, wo_copy(s, cross, 0, yflip, t)), hand(s, cross)]
+        + [(rim(h), wo_copy(s, cross, 1, at_z(h), t)) for h in (1, -1)])
     ev["wo_d"] = event(None, wo_copy(yflip, cross, 0, partner, t),
         [(ok, wo_copy(yflip, cross, 1, at_z(h), t)) for h, ok in ahead] + [hand(yflip, cross)])
-    ev["wo_d_end"] = event(None, None, [(ok, wo_copy(yflip, cross, 1, at_z(h), t)) for h, ok in ends])
+    def split_event(kind, d, arrival, items, at_rim=(), inner_only=()):
+        if abs(d) == 1:
+            ev[kind + "r", d] = event(rim(d), arrival, list(at_rim) + items)
+            ev[kind, d] = event(here(d) & jnp.logical_not(rim(d)), arrival, list(inner_only) + items)
+        else:
+            ev[kind, d] = event(None if d == 0 else here(d), arrival, list(inner_only) + items)
+
     for d in far:
         step, fine = onward(d)
         relay = 2 <= abs(d) < Z - 1
         b = at_z(d)
-        items = [(None, wo_copy(b, t, 0, s, cross)), (None, wo_copy(b, t, 0, yflip, t)), hand(b, t)]
+        to_x = [(None, wo_copy(b, t, 0, s, cross))]
+        items = [(None, wo_copy(b, t, 0, yflip, t)), hand(b, t)]
         if relay:
-            items = [(fine, wo_copy(b, t, 1, at_z(step), t))] + items
-        ev["w00", d] = event(here(d), wo_copy(b, t, 0, s, cross), items)
-        ev["w10", d] = event(here(d), wo_copy(b, cross, 0, partner, t), [hand(b, cross)])
+            to_x = [(fine, wo_copy(b, t, 1, at_z(step), t))] + to_x
+        split_event("w00", d, wo_copy(b, t, 0, s, cross), items, inner_only=to_x)
+        split_event("w10", d, wo_copy(b, cross, 0, partner, t), [hand(b, cross)],
+            [((z == 0) | (z == Z - 1), wo_copy(b, cross, 1, yflip, t))])
         b = at_yz(d)
         items = [hand(b, cross)]
         if relay:
             items = [(fine, wo_copy(b, cross, 1, at_z(step), t))] + items
-        ev["w11", d] = event(here(d), wo_copy(b, cross, 0, partner, t), items)
+        split_event("w11", d, wo_copy(b, cross, 0, partner, t), items)
     for d in [0] + far:
         b = at_yz(d)
-        ev["w01", d] = event(None if d == 0 else here(d), wo_copy(b, t, 0, partner, t), [hand(b, t)])
+        split_event("w01", d, wo_copy(b, t, 0, partner, t), [hand(b, t)])
 
     def poll(kind, *distances):
         for k in distances:
@@ -574,13 +586,15 @@
     key_value(0)
     key_value(chunks - 1)
     start_all(halo_kv)
-    poll("w00", 2)
-    ev["wo_d"]()
-    poll("w00", 1)
+    def early_relays():
+        poll("w00", 2)
+        ev["wo_d"]()
+        poll("w00r", 1)
+        poll("w00", 1)
+
+    early_relays()
     for i in range(1, chunks - 1):
         key_value(i)
-    ev["wo_d_end"]()
-
     span = QB + 2 * WINDOW
     row_id = lax.broadcasted_iota(jnp.int32, (QB, span), 0)
     col_id = lax.broadcasted_iota(jnp.int32, (QB, span), 1)
@@ -621,6 +635,14 @@
             att_send[pl.ds(at, QB), g * LANES:(g + 1) * LANES] = value
         ex_att(n).start()
 
+        @pl.when(i == 0)
+        def _():
+            poll("w10r", 1)
+
+        @pl.when(i == 1)
+        def _():
+            poll("w01", 0)
+
         return carry
 
     def attend_own(i, carry):
@@ -629,15 +651,13 @@
         for g, value in enumerate(attend(b)):
             joined[t, pl.ds(at, QB), g * LANES:(g + 1) * LANES] = value
 
-        @pl.when(i == 0)
+        @pl.when(i == 1)
         def _():
             poll("w00", *range(3, Z))
 
-        @pl.when(i == 2)
-        def _():
-            poll("w01", 0)
+        @pl.when(i == jnp.where((z == 0) | (z == Z - 1), 3, 2))
+        def _():
             poll("w11", 2)
-
         return carry
 
     lax.fori_loop(0, hb, attend_other, 0)
@@ -650,8 +670,19 @@
         at = pl.ds(pl.multiple_of(start, wide), count)
         return jnp.concatenate([wfull[2 * n, half, at, :], wfull[2 * n + 1, half, at, :]], axis=1)
 
+    at_rim = (z == 0) | (z == Z - 1)
+
+    def near():
+        poll("w01r", 1)
+        poll("w11r", 1)
+
+    def second():
+        poll("w01", 2)
+        poll("w10", 2)
+
     def pair_of(p):
-        zz = jnp.where(z < Z // 2, (z + p) % Z, (z + Z - p) % Z)
+        q = jnp.where(at_rim & ((p == 1) | (p == 2)), 3 - p, p)
+        zz = sum(((z // bit + q // bit) % 2) * bit for bit in [2 ** k for k in range(Z.bit_length() - 1)])
         return [zz * 2 + y, zz * 2 + 1 - y]
 
     def pair_wait(pair):
@@ -667,9 +698,8 @@
     def most(p, carry):
         @pl.when(p == 1)
         def _():
-            poll("w10", 1)
-            poll("w11", 1)
-            poll("w01", 1)
+            pl.when(at_rim)(second)
+            pl.when(jnp.logical_not(at_rim))(near)
         pair = pair_of(p)
         pair_wait(pair)
         left = jnp.concatenate([joined[t]] + [joined[T + k] for k in range(T)], axis=1)
@@ -691,6 +721,10 @@
     def whole(p, carry):
         @pl.when(p == split)
         def _():
+            poll("w10", 1)
+            poll("w11", 1)
+            poll("w01", 1)
+            poll("w01", *range(3, Z))
             poll("w10", *range(3, Z))
             poll("w11", *range(3, Z))
         pair = pair_of(p)
@@ -704,8 +738,8 @@
 
     split = Z // 2
     lax.fori_loop(0, split, most, 0)
-    poll("w01", *range(2, Z))
-    poll("w10", 2)
+    pl.when(at_rim)(near)
+    pl.when(jnp.logical_not(at_rim))(second)
     whole_att.wait_recv()
     lax.fori_loop(0, split, last, 0)
     lax.fori_loop(split, Z, whole, 0)
@@ -720,16 +754,21 @@
     whole_pool.wait_send()
     whole_att.wait_send()
     sent(kvw.at[pl.ds(0, 4 * Z - 1)], kv_send.at[0])
-    sent(wfull.at[s, t], wo_send.at[2])
-    sent(wfull.at[pl.ds(0, 3 * Z)], wo_send.at[0])
+    sent(wfull.at[s], wo_send.at[2])
+    sent(wfull.at[pl.ds(0, 3 * Z - 1)], wo_send.at[0])
     for at in range(Z):
         inside = lambda k: 0 <= k < Z
+        edge = (0, Z - 1)
         count = sum(inside(at + h) for h in hop)
-        count += sum(inside(at + d) and inside(at - d // abs(d)) for d in far if 2 <= abs(d) < Z - 1)
+        count += sum(inside(at + h) and (abs(h) > 1 or inside(at + 2 * h)) for h in hop)
+        count += 2 * sum(inside(at + d) and inside(at - d // abs(d)) for d in far if 2 <= abs(d) < Z - 1)
+        for h in (1, -1):
+            if inside(at + h):
+                count += (at in edge or at + h in edge) + (at in edge)
 
         @pl.when(z == at)
         def _(count=count):
-            sent(wfull.at[pl.ds(0, count)], wo_send.at[1])
+            sent(wfull.at[pl.ds(0, count // 2)], wo_send.at[1])
 
 
 def body(mesh, tokens, norm_gain, w_query, w_key, w_value, w_pool_in, sink_logit, pool_scale, w_out):
@@ -738,7 +777,7 @@
     rows, width = tokens.shape
     local_heads = w_query.shape[1] // HEAD
     fits = (
-        S % 4 == 0 and S > 4 and T == 2
+        S % 4 == 0 and S > 4 and S & (S - 1) == 0 and T == 2
         and w_out.shape[1] == LANES and w_key.shape == (LANES, LANES) and w_value.shape == w_key.shape
         and w_query.shape[1] % LANES == 0 and w_pool_in.shape[1] % LANES == 0
         and w_query.shape[1] == w_pool_in.shape[1]

time: 36.5 us -> 34.7 us (0.951)
  Pallas kernels: 35 us -> 32.9 us
    pallas_call x1, Pallas kernels: 35 us -> 32.9 us  [body(): pl.pallas_call(functools.partial(mixer_kernel, (S, T)), out_shape=pltpu.V...]
where the time goes in v5:
time: 34.7 us; the launch traced here: 34.2 us
  Pallas kernels  32.9 us (95%)
  local copies, waits for them, and re-layouts  1.32 us (4%)
    pallas_call x1, Pallas kernels, body(): pl.pallas_call(functools.partial(mixer_kernel, (S, T)), out_shape=pltpu.V...  32.9 us
    unnamed x1, local copies, waits for them, and re-layouts  1.32 us

profile of v5, /device:TPU:0, one launch (start us, length us, event | category | flops | bytes accessed | tf_op | source)
XLA Modules:
  0.0 34.2 jit_solution(16591021701746972296)
XLA Ops:
  0.0 32.9 %shard_map.127 = bf16[512,2048]{1,0:T(8,128)(2,1)S(1)} custom-call(bf16[1024,2048]{1,0:T(8,128)(2,1)} %tokens.1, f32[16,128]{1,0:T(8,128)} %bitcast.2, bf16[2048,256]{1,0:T(8,128)(2,1)} %w_query.1, bf16[128,128]{1,0:T(8,128)(2,1)} %w_key.1, bf16[128,128]{1,0:T(8,128)(2,1)} %w_value.1, bf16[2048,256]{1,0:T(8,128)(2,1)} %w_pool.1, f32[4]{0:T(128)} %sink.1, ...), custom_call_target="tpu_custom_call" | custom-call | tf_op jit(solution)/shard_map/pallas_call | solution.py:801
  32.9 1.3 %copy.15 = bf16[512,2048]{1,0:T(8,128)(2,1)} copy(bf16[512,2048]{1,0:T(8,128)(2,1)S(1)} %shard_map.127) | data formatting | bytes 4194304

commit v6 on v5

--- a/solution.py
+++ b/solution.py
@@ -341,8 +341,16 @@
         to_x = [(None, wo_copy(b, t, 0, s, cross))]
         items = [(None, wo_copy(b, t, 0, yflip, t)), hand(b, t)]
         if relay:
-            to_x = [(fine, wo_copy(b, t, 1, at_z(step), t))] + to_x
-        split_event("w00", d, wo_copy(b, t, 0, s, cross), items, inner_only=to_x)
+            served = here(d) & fine
+            arrival = wo_copy(b, t, 0, s, cross)
+            busy = (c == 0) & (y == 0) if step < 0 else (c == 1) & (y == 1)
+            forward = [(None, wo_copy(b, t, 1, at_z(step), t))]
+            ev["relay", d] = event(served & jnp.logical_not(busy), arrival, forward)
+            ev["relay_late", d] = event(served & busy, arrival, forward)
+            ev["served", d] = event(served, None, to_x + items)
+            ev["w00", d] = event(here(d) & jnp.logical_not(fine), arrival, to_x + items)
+        else:
+            split_event("w00", d, wo_copy(b, t, 0, s, cross), items, inner_only=to_x)
         split_event("w10", d, wo_copy(b, cross, 0, partner, t), [hand(b, cross)],
             [((z == 0) | (z == Z - 1), wo_copy(b, cross, 1, yflip, t))])
         b = at_yz(d)
@@ -518,21 +526,24 @@
         def _():
             begin()
 
-        @pl.when(i == jnp.where(z == 0, 1, 0))
+        @pl.when(i == 1)
         def _():
             ev["wo_own_z"]()
 
-        @pl.when(i == hc - 1)
-        def _():
-            for n in range(1, hb - 1):
-                send_pooled(n)
-
-        @pl.when(i == hc)
-        def _():
-            send_pooled(jnp.where(t == 0, 0, hb - 1))
+        @pl.when(i == jnp.where((z == 0) | (z == Z - 1), hc, hc - 1))
+        def _():
             kv_wait(0, Z - 1)
             start_all(kv_to_y)
             start_all(kv_to_p)
+
+        @pl.when(i == hc - 1)
+        def _():
+            for n in range(1, hb - 1):
+                send_pooled(n)
+
+        @pl.when(i == hc)
+        def _():
+            send_pooled(jnp.where(t == 0, 0, hb - 1))
             ev["wo_own_end"]()
 
         @pl.when(i == jnp.where(z == 0, chunks - 1, hc))
@@ -564,6 +575,7 @@
     kv_wait(1, Z)
     start_all(kv_y_to_p)
     kv_wait(2, 2 * Z)
+    poll("relay", 2)
 
     def gather_sum(b, carry):
         return carry + jnp.sum(kvw[b].astype(jnp.float32).reshape(LANES // 8, 8, LANES), axis=0)
@@ -587,6 +599,8 @@
     key_value(chunks - 1)
     start_all(halo_kv)
     def early_relays():
+        poll("relay_late", 2)
+        poll("served", 2)
         poll("w00", 2)
         ev["wo_d"]()
         poll("w00r", 1)
@@ -651,7 +665,7 @@
         for g, value in enumerate(attend(b)):
             joined[t, pl.ds(at, QB), g * LANES:(g + 1) * LANES] = value
 
-        @pl.when(i == 1)
+        @pl.when(i == 2)
         def _():
             poll("w00", *range(3, Z))
 

time: 34.7 us -> 34.7 us (level)
  no operation moved by 1% of the time
where the time goes in v6:
time: 34.7 us; the launch traced here: 34 us
  Pallas kernels  32.7 us (94%)
  local copies, waits for them, and re-layouts  1.32 us (4%)
    pallas_call x1, Pallas kernels, body(): pl.pallas_call(functools.partial(mixer_kernel, (S, T)), out_shape=pltpu.V...  32.7 us
    unnamed x1, local copies, waits for them, and re-layouts  1.32 us

profile of v6, /device:TPU:0, one launch (start us, length us, event | category | flops | bytes accessed | tf_op | source)
XLA Modules:
  0.0 34.0 jit_solution(2940939006100432044)
XLA Ops:
  0.0 32.7 %shard_map.127 = bf16[512,2048]{1,0:T(8,128)(2,1)S(1)} custom-call(bf16[1024,2048]{1,0:T(8,128)(2,1)} %tokens.1, f32[16,128]{1,0:T(8,128)} %bitcast.2, bf16[2048,256]{1,0:T(8,128)(2,1)} %w_query.1, bf16[128,128]{1,0:T(8,128)(2,1)} %w_key.1, bf16[128,128]{1,0:T(8,128)(2,1)} %w_value.1, bf16[2048,256]{1,0:T(8,128)(2,1)} %w_pool.1, f32[4]{0:T(128)} %sink.1, ...), custom_call_target="tpu_custom_call" | custom-call | tf_op jit(solution)/shard_map/pallas_call | solution.py:815
  32.7 1.3 %copy.15 = bf16[512,2048]{1,0:T(8,128)(2,1)} copy(bf16[512,2048]{1,0:T(8,128)(2,1)S(1)} %shard_map.127) | data formatting | bytes 4194304

commit v7 on v5

--- a/solution.py
+++ b/solution.py
@@ -223,7 +223,7 @@
     ]
     barrier = pltpu.get_barrier_semaphore()
     greet = [(((z + d) % Z) * 4 + s % 4, t) for d in range(1, Z)]
-    greet += [(yflip, t), (after, t), (before, t), (s, cross), (yflip, cross)]
+    greet += [(yflip, t), (after, t), (before, t), (s, cross)]
     for to_s, to_t in greet:
         pl.semaphore_signal(barrier, inc=1, device_id={"sp": to_s, "tp": to_t}, device_id_type=MESH)
     for copy in own_copies[:6]:

time: 34.7 us -> 34.7 us (level)
  no operation moved by 1% of the time
where the time goes in v7:
time: 34.7 us; the launch traced here: 34 us
  Pallas kernels  32.7 us (94%)
  local copies, waits for them, and re-layouts  1.32 us (4%)
    pallas_call x1, Pallas kernels, body(): pl.pallas_call(functools.partial(mixer_kernel, (S, T)), out_shape=pltpu.V...  32.7 us
    unnamed x1, local copies, waits for them, and re-layouts  1.32 us

profile of v7, /device:TPU:0, one launch (start us, length us, event | category | flops | bytes accessed | tf_op | source)
XLA Modules:
  0.0 34.0 jit_solution(17279991087338355011)
XLA Ops:
  0.0 32.7 %shard_map.127 = bf16[512,2048]{1,0:T(8,128)(2,1)S(1)} custom-call(bf16[1024,2048]{1,0:T(8,128)(2,1)} %tokens.1, f32[16,128]{1,0:T(8,128)} %bitcast.2, bf16[2048,256]{1,0:T(8,128)(2,1)} %w_query.1, bf16[128,128]{1,0:T(8,128)(2,1)} %w_key.1, bf16[128,128]{1,0:T(8,128)(2,1)} %w_value.1, bf16[2048,256]{1,0:T(8,128)(2,1)} %w_pool.1, f32[4]{0:T(128)} %sink.1, ...), custom_call_target="tpu_custom_call" | custom-call | tf_op jit(solution)/shard_map/pallas_call | solution.py:801
  32.7 1.3 %copy.15 = bf16[512,2048]{1,0:T(8,128)(2,1)} copy(bf16[512,2048]{1,0:T(8,128)(2,1)S(1)} %shard_map.127) | data formatting | bytes 4194304
